TPU v7x, 32 devices: a whole 2x2x4 slice. The times are simulated.
32 devices in a mesh: ep: 4 (over y, x), tp: 8 (over z, core).
Axes of the slice: x: 2, y: 2, z: 4, core: 2. Of those that a mesh axis runs over, the one named last changes fastest.
Arguments:
- mixer_input: bfloat16 [6144, 1024], P(('ep', 'tp')), may hold values from -6 to 6
- mixer_gain: float32 [1024], replicated, may hold values from 0.1 to 1.9
- group_weight: bfloat16 [4, 256, 256], replicated, may hold values from -0.375 to 0.375
- mixer_scale: float32 [1024], replicated, may hold values from 0.1 to 1.9
- expert_input: bfloat16 [6144, 1024], P(('ep', 'tp')), may hold values from -6 to 6
- expert_gain: float32 [1024], replicated, may hold values from 0.1 to 1.9
- routes: int32 [6144, 2], P(('ep', 'tp')), may hold values from 0 to 3, all different within a row; in each aligned block of 192 rows (0 to 191, 192 to 383, ...) at most 144 rows name the same one
- route_weight: float32 [6144, 2], P(('ep', 'tp')), may hold values from 0.2 to 1
- w_gate: bfloat16 [4, 1024, 4096], P('ep', None, 'tp'), may hold values from -0.1875 to 0.1875
- w_up: bfloat16 [4, 1024, 4096], P('ep', None, 'tp'), may hold values from -0.1875 to 0.1875
- w_down: bfloat16 [4, 4096, 1024], P('ep', 'tp'), may hold values from -0.09375 to 0.09375
Outputs:
- mixer_out: bfloat16 [6144, 1024], P(('ep', 'tp'))
- expert_out: bfloat16 [6144, 1024], P(('ep', 'tp'))
Inputs may be any that keep to these rules, and one draw needn't show every extreme that they name: `routes`: each row names 2 different experts. Among the rows of one device no expert is named by more than 144 rows, and in some device's rows some expert is named exactly 144 times.
All inputs are finite; a program needn't handle non-finite values.
Results may differ from a plain program's by a relative error of at most 0.0076.
Values may be sent and summed in bfloat16 or wider, within the bound.
A program may use at most 128 MiB of HBM per device.

v0:
```python
import functools

import jax
import jax.numpy as jnp
from jax import lax
from jax.experimental import pallas as pl
from jax.experimental.pallas import tpu as pltpu
from jax.sharding import PartitionSpec as P

epsilon = 1e-06
vmem_share = 2**24


def padded_2(value, sides, width):
    for axis, dim in sides:
        size, length = (lax.axis_size(axis), value.shape[dim])
        up = [(i, (i + 1) % size) for i in range(size - 1)]
        down = [(j, i) for i, j in up]
        last = lax.slice_in_dim(value, length - width, length, axis=dim)
        leading = lax.slice_in_dim(value, 0, width, axis=dim)
        before = lax.ppermute(last, axis, up)
        after = lax.ppermute(leading, axis, down)
        value = jnp.concatenate([before, value, after], axis=dim)
    return value


def normalize(row_values, gain):
    values = row_values.astype(jnp.float32)
    scaled = values * lax.rsqrt(jnp.mean(values * values, axis=-1, keepdims=True) + epsilon)
    return (scaled * gain).astype(jnp.bfloat16)


def pool_groups(padded, start_row, row_count, seq_length):
    group_width = padded.shape[1] // 4
    position = start_row + jnp.arange(row_count, dtype=jnp.int32)
    centre = padded[8 : 8 + row_count]
    pooled_parts = []
    for group_index in range(4):
        window = 2 ** (group_index + 1)
        reach_left = window // 2
        reach_right = window - 1 - reach_left
        group_cols = padded[:, group_index * group_width : (group_index + 1) * group_width]
        window_sum = group_cols[8 - reach_left : 8 - reach_left + row_count]
        for offset in range(1 - reach_left, reach_right + 1):
            window_sum = window_sum + group_cols[8 + offset : 8 + offset + row_count]
        cover = (
            jnp.minimum(position + reach_right + 1, seq_length)
            - jnp.maximum(position - reach_left, 0)
        ).astype(jnp.float32)
        pooled_parts.append(
            window_sum / cover[:, None]
            - centre[:, group_index * group_width : (group_index + 1) * group_width]
        )
    return jnp.stack(pooled_parts, axis=1).astype(jnp.bfloat16)


def mixer(mixer_input, mixer_gain, group_weight, mixer_scale):
    row_count = mixer_input.shape[0]
    normed = normalize(mixer_input, mixer_gain)
    padded = padded_2(normed, ((("ep", "tp"), 0),), 8)
    start_row = lax.axis_index(("ep", "tp")) * row_count
    seq_length = row_count * lax.axis_size(("ep", "tp"))
    pooled = pool_groups(padded.astype(jnp.float32), start_row, row_count, seq_length)
    mixed_groups = jnp.einsum(
        "tgi,gio->tgo", pooled, group_weight, preferred_element_type=jnp.float32
    )
    return (mixed_groups.reshape(row_count, -1) * mixer_scale).astype(jnp.bfloat16)


def routed_plan(expert_input, expert_gain, routes, route_weight, w_gate, w_up, w_down):
    row_count = expert_input.shape[0]
    top_count = routes.shape[1]
    experts = lax.axis_size("ep") * w_gate.shape[0]
    capacity = 3 * top_count * row_count // (2 * experts)
    normed = normalize(expert_input, expert_gain)
    flat_route = routes.reshape(-1)
    onehot = (flat_route[:, None] == jnp.arange(experts, dtype=jnp.int32)[None, :]).astype(
        jnp.int32
    )
    before = jnp.cumsum(onehot, axis=0) - onehot
    slot_index = flat_route * capacity + jnp.sum(before * onehot, axis=1)
    places = (
        slot_index.reshape(row_count, top_count)[None, :, :]
        == jnp.arange(experts * capacity, dtype=jnp.int32)[:, None, None]
    )
    dispatch = jnp.any(places, axis=2).astype(jnp.bfloat16)
    outgoing = jnp.dot(dispatch, normed, preferred_element_type=jnp.float32).astype(jnp.bfloat16)
    arrived = lax.all_to_all(outgoing, "ep", split_axis=0, concat_axis=0, tiled=True)
    down_w = w_down[0]
    paired = jnp.stack((w_gate[0], w_up[0]), axis=0)
    portion = lax.all_gather(paired, "tp", axis=2, tiled=True)
    gate_part = jnp.dot(arrived, portion[0], preferred_element_type=jnp.float32)
    up_part = jnp.dot(arrived, portion[1], preferred_element_type=jnp.float32)
    hidden = (jax.nn.silu(gate_part) * up_part).astype(jnp.bfloat16)
    block_width = down_w.shape[0]
    portion = lax.all_gather(down_w, "tp", axis=0, tiled=True)
    blocks = portion.shape[0] // block_width
    hidden_part = hidden
    hidden_part = hidden_part.reshape(hidden_part.shape[0], blocks, block_width)
    block_terms = jnp.einsum(
        "rkf,kfd->krd",
        hidden_part,
        portion.reshape(blocks, block_width, portion.shape[1]),
        preferred_element_type=jnp.float32,
    )
    rounded = lax.optimization_barrier(block_terms.astype(jnp.bfloat16)).astype(jnp.float32)
    result = jnp.sum(rounded, axis=0)
    returned = lax.all_to_all(
        result.astype(jnp.bfloat16), "ep", split_axis=0, concat_axis=0, tiled=True
    )
    picked = (
        jnp.take(returned, slot_index, axis=0).astype(jnp.float32).reshape(row_count, top_count, -1)
    )
    expert_out = jnp.sum(picked * route_weight[:, :, None], axis=1).astype(jnp.bfloat16)
    return expert_out


def slots(routes, route_weight, experts):
    chosen = routes[:, :, None] == jnp.arange(experts, dtype=jnp.int32)[None, None, :]
    named = jnp.any(chosen, axis=1)
    weight = jnp.sum(jnp.where(chosen, route_weight[:, :, None], 0.0), axis=1)
    rows = routes.shape[0]
    earlier = jnp.arange(rows)[None, :] < jnp.arange(rows)[:, None]
    place = jnp.dot(
        earlier.astype(jnp.bfloat16), named.astype(jnp.bfloat16), preferred_element_type=jnp.float32
    )
    place = jnp.where(named, place, -1.0)
    high = lax.reduce_precision(weight, 8, 7)
    return jnp.concatenate([place, high, weight - high], axis=1).T.astype(jnp.bfloat16)


def near_first(length):
    return [sorted(range(length), key=lambda other: abs(other - at)) for at in range(length)]


def stream_kernel(
    depth, capacity, experts,
    token_ref, gate_ref, up_ref, down_ref, out_ref,
    tok, res, from_core, half_low, half_high, from_right, from_left, from_above, from_below,
    send_sem, recv_sem, local_sem,
):
    column, line = lax.axis_index("ep"), lax.axis_index("tp")
    level, core = line // 2, line % 2
    other = 1 - core
    tall = token_ref.shape[0]
    rows = out_ref.shape[0]
    half = rows // 2
    right_column, left_column = (2 * column + 1) % 5, (3 * column + 2) % 5
    right, left = (right_column, line), (left_column, line)
    beside = (column, level * 2 + other)
    above, below = (column, line + 2), (column, line - 2)
    has_above, has_below = level < depth - 1, level > 0

    def level_of(step):
        value = 0
        for at, order in enumerate(near_first(depth)):
            for turn, there in enumerate(order):
                value = value + there * jnp.where((level == at) & (step == turn), 1, 0)
        return value

    def link(src, dst, kind, at, target):
        return pltpu.make_async_remote_copy(
            src_ref=src, dst_ref=dst, send_sem=send_sem.at[kind, at],
            recv_sem=recv_sem.at[kind, at], device_id=target,
            device_id_type=pl.DeviceIdType.MESH,
        )

    def up(at):
        return link(tok.at[at, 0, core], tok.at[at, 0, core], 0, at, above)

    def down(at):
        return link(tok.at[at, 0, core], tok.at[at, 0, core], 1, at, below)

    def to_right(at):
        return link(tok.at[at, 0, core], tok.at[at, 1, core], 2, at, right)

    def to_left(at):
        return link(tok.at[at, 0, core], tok.at[at, 2, core], 3, at, left)

    def on_right(at):
        part = pl.ds(0, half)
        return link(tok.at[at, 1, core, part], tok.at[at, 3, core, part], 4, at, right)

    def on_left(at):
        part = pl.ds(half, tall - half)
        return link(tok.at[at, 2, core, part], tok.at[at, 3, core, part], 5, at, left)

    def share(at, q):
        return link(tok.at[at, q, core], tok.at[at, q, core], 6 + q, at, beside)

    def shared_in(at, q):
        return link(tok.at[at, q, other], tok.at[at, q, other], 6 + q, at, beside)

    def give(at, q):
        return link(res.at[at, q, other], from_core.at[at, q], 10 + q, at, beside)

    def back_low(at):
        return link(res.at[at, 3, core, pl.ds(0, half)], half_low.at[at], 14, at, left)

    def back_high(at):
        return link(res.at[at, 3, core, pl.ds(half, half)], half_high.at[at], 15, at, right)

    def back_left(at):
        return link(res.at[at, 1, core], from_right.at[at], 16, at, left)

    def back_right(at):
        return link(res.at[at, 2, core], from_left.at[at], 17, at, right)

    def back_down(at):
        return link(res.at[at, 0, core], from_above.at[at], 18, at, below)

    def back_up(at):
        return link(res.at[at, 0, core], from_below.at[at], 19, at, above)

    barrier = pltpu.get_barrier_semaphore()

    def greet(target):
        pl.semaphore_signal(
            barrier, inc=1, device_id=target, device_id_type=pl.DeviceIdType.MESH
        )

    greet(right)
    greet(left)
    greet(beside)
    pl.when(has_above)(lambda: greet(above))
    pl.when(has_below)(lambda: greet(below))
    own_copy = pltpu.make_async_copy(token_ref, tok.at[level, 0, core], local_sem)
    own_copy.start()
    own_copy.wait()
    pl.semaphore_wait(barrier, 3 + jnp.where(has_above, 1, 0) + jnp.where(has_below, 1, 0))

    piece = half // 3 if half % 48 == 0 else half
    f32 = jnp.float32

    def add(at, q, start, count, terms):
        def body(i, carry):
            span = pl.ds(pl.multiple_of(start + i * piece, piece), piece)
            there = pl.ds(pl.multiple_of(i * piece, piece), piece)
            total = res[at, q, core, span].astype(f32) + from_core[at, q, span].astype(f32)
            for term in terms:
                total = total + term[at, there].astype(f32)
            res[at, q, core, span] = total.astype(jnp.bfloat16)
            return carry

        lax.fori_loop(0, count // piece, body, 0)

    def corner(at):
        give(at, 3).wait_recv()
        add(at, 3, 0, rows, [])
        back_low(at).start()
        back_high(at).start()

    def compute(at, q):
        picks, scales, chosen = [], [], []
        for lane in range(2):
            listed = tok[at, q, lane, pl.ds(rows, tall - rows), pl.ds(0, rows)].astype(f32)
            listing = lax.broadcasted_iota(jnp.int32, listed.shape, 0)

            def row_of(index):
                return jnp.sum(jnp.where(listing == index, listed, 0.0), axis=0, keepdims=True)

            weight = row_of(experts + column) + row_of(2 * experts + column)
            index = lax.broadcasted_iota(jnp.int32, (capacity, rows), 0).astype(jnp.float32)
            hit = index == row_of(column)
            scales.append(jnp.sum(jnp.where(hit, weight, 0.0), axis=1, keepdims=True))
            picks.append(jnp.where(hit, 1.0, 0.0).astype(jnp.bfloat16))
            chosen.append(
                jnp.dot(picks[lane], tok[at, q, lane, pl.ds(0, rows)], preferred_element_type=jnp.float32)
                .astype(jnp.bfloat16)
            )
        gathered = jnp.concatenate(chosen, axis=0)
        gate_part = jnp.dot(gathered, gate_ref[...], preferred_element_type=jnp.float32)
        up_part = jnp.dot(gathered, up_ref[...], preferred_element_type=jnp.float32)
        hidden = (gate_part / (1.0 + jnp.exp(-gate_part)) * up_part).astype(jnp.bfloat16)
        partial = jnp.dot(hidden, down_ref[...], preferred_element_type=jnp.float32)
        partial = (partial * jnp.concatenate(scales, axis=0)).astype(jnp.bfloat16)
        for lane in range(2):
            res[at, q, lane] = lax.dot_general(
                picks[lane], partial[lane * capacity : (lane + 1) * capacity],
                (((0,), (0,)), ((), ())), preferred_element_type=jnp.float32,
            ).astype(jnp.bfloat16)

    def stage(turn, carry):
        @pl.when(turn < depth)
        def _():
            at = level_of(turn)
            pl.when(at < level)(lambda: up(at).wait_recv())
            pl.when(at > level)(lambda: down(at).wait_recv())
            pl.when((at <= level) & has_above)(lambda: up(at).start())
            pl.when((at >= level) & has_below)(lambda: down(at).start())
            to_right(at).start()
            to_left(at).start()
            share(at, 0).start()

        @pl.when((turn >= 1) & (turn < depth + 1))
        def _():
            at = level_of(turn - 1)
            to_right(at).wait_recv()
            on_right(at).start()
            share(at, 1).start()
            to_left(at).wait_recv()
            on_left(at).start()
            share(at, 2).start()

        @pl.when((turn >= 2) & (turn < depth + 2))
        def _():
            at = level_of(turn - 2)
            on_right(at).wait_recv()
            on_left(at).wait_recv()
            share(at, 3).start()

        pl.when(turn >= 3)(lambda: corner(level_of(turn - 3)))

        def one(q, inner):
            step = turn - (q + 1) // 2

            @pl.when((step >= 0) & (step < depth))
            def _():
                at = level_of(step)
                shared_in(at, q).wait_recv()
                compute(at, q)
                give(at, q).start()

            return inner

        lax.fori_loop(0, 4, one, 0)
        return carry

    lax.fori_loop(0, depth + 3, stage, 0)

    def extend(at, term):
        def body(i, carry):
            span = pl.ds(pl.multiple_of(i * piece, piece), piece)
            res[at, 0, core, span] = (
                res[at, 0, core, span].astype(f32) + term[at, span].astype(f32)
            ).astype(jnp.bfloat16)
            return carry

        lax.fori_loop(0, rows // piece, body, 0)

    def sides(at):
        give(at, 1).wait_recv()
        back_low(at).wait_recv()
        add(at, 1, 0, half, [half_low])
        add(at, 1, half, half, [])
        back_left(at).start()
        give(at, 2).wait_recv()
        back_high(at).wait_recv()
        add(at, 2, 0, half, [])
        add(at, 2, half, half, [half_high])
        back_right(at).start()

    def home(at):
        give(at, 0).wait_recv()
        back_left(at).wait_recv()
        back_right(at).wait_recv()
        add(at, 0, 0, rows, [from_right, from_left])

        @pl.when((at <= level) & has_above)
        def _():
            back_down(at).wait_recv()
            extend(at, from_above)

        @pl.when((at >= level) & has_below)
        def _():
            back_up(at).wait_recv()
            extend(at, from_below)

        pl.when(at < level)(lambda: back_down(at).start())
        pl.when(at > level)(lambda: back_up(at).start())

    def finish(turn, carry):
        pl.when(turn < depth)(lambda: sides(level_of(depth - 1 - turn)))
        pl.when(turn >= 1)(lambda: home(level_of(depth - turn)))
        return carry

    lax.fori_loop(0, depth + 1, finish, 0)
    out_copy = pltpu.make_async_copy(res.at[level, 0, core], out_ref, local_sem)
    out_copy.start()

    def drain(at, carry):
        pl.when((at <= level) & has_above)(lambda: up(at).wait_send())
        pl.when((at >= level) & has_below)(lambda: down(at).wait_send())
        for copy in (to_right, to_left, on_right, on_left):
            copy(at).wait_send()
        for copy in (back_low, back_high, back_left, back_right):
            copy(at).wait_send()
        for q in range(4):
            share(at, q).wait_send()
            give(at, q).wait_send()
        pl.when(at < level)(lambda: back_down(at).wait_send())
        pl.when(at > level)(lambda: back_up(at).wait_send())
        return carry

    lax.fori_loop(0, depth, drain, 0)
    out_copy.wait()


def dense_plan(expert_input, expert_gain, routes, route_weight, w_gate, w_up, w_down):
    row_count, width = expert_input.shape
    experts = lax.axis_size("ep")
    depth = lax.axis_size("tp") // 2
    capacity = 3 * routes.shape[1] * row_count // (2 * experts)
    normed = normalize(expert_input, expert_gain)
    listed = slots(routes, route_weight, experts)
    pad = -(-3 * experts // 16) * 16
    listed = jnp.pad(listed, ((0, pad - 3 * experts), (0, width - row_count)))
    sent = jnp.concatenate([normed, listed], axis=0)
    bf16 = jnp.bfloat16
    half = row_count // 2
    vmem = pl.BlockSpec(memory_space=pltpu.VMEM)
    return pl.pallas_call(
        functools.partial(stream_kernel, depth, capacity, experts),
        out_shape=jax.ShapeDtypeStruct((row_count, width), bf16),
        in_specs=[vmem] * 4,
        out_specs=vmem,
        scratch_shapes=[
            pltpu.VMEM((depth, 4, 2, row_count + pad, width), bf16),
            pltpu.VMEM((depth, 4, 2, row_count, width), bf16),
            pltpu.VMEM((depth, 4, row_count, width), bf16),
            pltpu.VMEM((depth, half, width), bf16),
            pltpu.VMEM((depth, half, width), bf16),
            pltpu.VMEM((depth, row_count, width), bf16),
            pltpu.VMEM((depth, row_count, width), bf16),
            pltpu.VMEM((depth, row_count, width), bf16),
            pltpu.VMEM((depth, row_count, width), bf16),
            pltpu.SemaphoreType.DMA((20, depth)),
            pltpu.SemaphoreType.DMA((20, depth)),
            pltpu.SemaphoreType.DMA,
        ],
        compiler_params=pltpu.CompilerParams(
            collective_id=0, has_side_effects=True, vmem_limit_bytes=60 * 2**20
        ),
    )(sent, w_gate[0], w_up[0], w_down[0])


def on_device(
    mixer_input, mixer_gain, group_weight, mixer_scale,
    expert_input, expert_gain, routes, route_weight, w_gate, w_up, w_down,
):
    devices = lax.axis_size(("ep", "tp"))
    gathered_bytes = 2 * devices * expert_input.size
    square = lax.axis_size("ep") == 4
    plan = dense_plan if square and gathered_bytes <= vmem_share else routed_plan
    expert_out = plan(expert_input, expert_gain, routes, route_weight, w_gate, w_up, w_down)
    return (mixer(mixer_input, mixer_gain, group_weight, mixer_scale), expert_out)


def solution(mesh):
    placed = (
        P(("ep", "tp"), None),
        P(),
        P(),
        P(),
        P(("ep", "tp"), None),
        P(),
        P(("ep", "tp"), None),
        P(("ep", "tp"), None),
        P("ep", None, "tp"),
        P("ep", None, "tp"),
        P("ep", "tp", None),
    )
    return jax.shard_map(
        on_device,
        mesh=mesh,
        in_specs=placed,
        out_specs=(P(("ep", "tp"), None), P(("ep", "tp"), None)),
        check_vma=False,
    )
```

profile of v0, /device:TPU:0, one launch (start us, length us, event | category | flops | bytes accessed | tf_op | source)
XLA Modules:
  0.0 143.1 jit_solution(18363904212054140669)
XLA Ops:
  0.6 0.0 copy-start
  0.6 0.0 copy-start.1
  0.7 1.2 fusion.2
  1.9 0.0 copy-done.1
  1.9 0.0 copy-start.2
  1.9 0.9 fusion.4
  2.8 2.4 %collective-permute-start = (bf16[8,1024]{1,0:T(8,128)(2,1)S(1)}, bf16[8,1024]{1,0:T(8,128)(2,1)S(1)}, u32[]{:S(2)}, u32[]{:S(2)}) collective-permute-start(bf16[8,1024]{1,0:T(8,128)(2,1)S(1)} %get-tuple-element.5), channel_id=1, source_target_pairs={{0,1},{1,2},{2,3},{3,4},{4,5},{5,6},{6,7},{7,8},{8,9},{9,10},{10,1... | collective-permute-start | bytes 49160 | tf_op jit(solution)/shard_map/ppermute | solution.py:21
  5.2 1.3 collective-permute-start.1
  6.5 0.0 copy-start.4
  6.6 0.7 copy-done.4
  7.2 0.0 copy-start.7
  7.2 0.7 copy-done.7
  7.9 0.1 fusion
  8.1 0.0 copy-done.2
  8.1 0.2 fusion.5
  8.3 0.5 copy-done.5
  8.8 0.2 fusion.7
  9.0 0.8 fusion.8.token_ref
  9.8 129.9 %shard_map.122 = bf16[192,1024]{1,0:T(8,128)(2,1)} custom-call(bf16[208,1024]{1,0:T(8,128)(2,1)} %fusion.8.token_ref, bf16[1024,512]{1,0:T(8,128)(2,1)} %bitcast.20, bf16[1024,512]{1,0:T(8,128)(2,1)} %bitcast.21, bf16[512,1024]{1,0:T(8,128)(2,1)} %bitcast.22), custom_call_target="tpu_custom_call" | custom-call | tf_op jit(solution)/shard_map/pallas_call | solution.py:412
  139.7 0.0 collective-permute-done
  139.7 0.0 collective-permute-done.1
  139.7 0.1 maximum_convert_fusion
  139.8 0.2 fusion.34
  140.0 0.3 fusion.31
  140.3 0.0 copy-done
  140.3 0.3 convolution_bitcast_fusion
  140.6 0.0 copy-start.6
  140.6 0.1 copy.19
  140.7 0.6 copy-done.6
  141.3 0.8 multiply_convert_fusion
  142.1 0.2 copy-done.3
  142.4 0.7 copy.21
  (11 shorter events, 0.1 us)
Async XLA Ops:
  0.6 139.7 %copy-start = (bf16[4,256,256]{2,1,0:T(8,128)(2,1)S(1)}, bf16[4,256,256]{2,1,0:T(8,128)(2,1)}, u32[]{:S(2)}) copy-start(bf16[4,256,256]{2,1,0:T(8,128)(2,1)} %param.13) | copy-start | bytes 1572868
  0.6 1.3 copy-start.1
  1.9 6.2 %copy-start.2 = (bf16[192,1024]{1,0:T(8,128)(2,1)S(1)}, bf16[192,1024]{1,0:T(8,128)(2,1)}, u32[]{:S(2)}) copy-start(bf16[192,1024]{1,0:T(8,128)(2,1)} %param.15) | copy-start | bytes 1179652
  2.8 136.8 %collective-permute-start = (bf16[8,1024]{1,0:T(8,128)(2,1)S(1)}, bf16[8,1024]{1,0:T(8,128)(2,1)S(1)}, u32[]{:S(2)}, u32[]{:S(2)}) collective-permute-start(bf16[8,1024]{1,0:T(8,128)(2,1)S(1)} %get-tuple-element.5), channel_id=1, source_target_pairs={{0,1},{1,2},{2,3},{3,4},{4,5},{5,6},{6,7},{7,8},{8,9},{9,10},{10,1... | collective-permute-start | bytes 49160 | tf_op jit(solution)/shard_map/ppermute | solution.py:21
  5.2 134.5 %collective-permute-start.1 = (bf16[8,1024]{1,0:T(8,128)(2,1)S(1)}, bf16[8,1024]{1,0:T(8,128)(2,1)S(1)}, u32[]{:S(2)}, u32[]{:S(2)}) collective-permute-start(bf16[8,1024]{1,0:T(8,128)(2,1)S(1)} %get-tuple-element.6), channel_id=1, source_target_pairs={{1,0},{2,1},{3,2},{4,3},{5,4},{6,5},{7,6},{8,7},{9,8},{10,9},{11,1... | collective-permute-start | bytes 49160 | tf_op jit(solution)/shard_map/ppermute | solution.py:22
  6.5 0.7 copy-start.4
  7.2 0.7 copy-start.7
  8.1 0.7 copy-start.5
  140.6 0.7 copy-start.6
  141.3 1.1 copy-start.3
where the time goes:
time: 143 us
  Pallas kernels  130 us (91%)
  other arithmetic  4.74 us (3%)
  starting transfers between devices  3.69 us (3%)
  local copies, waits for them, and re-layouts  3.54 us (2%)
    pallas_call x1, Pallas kernels, dense_plan(): pl.pallas_call(functools.partial(stream_kernel, depth, capacity, experts)...  130 us
    unnamed x17, local copies, waits for them, and re-layouts  3.46 us
  transfers between devices with their start and end apart: 2, of which 0 were waited for; matrix products, arithmetic and copies ran while one was open for 1% of the time, Pallas kernels for 91%

commit v1 on v0

v1 whole, which is shorter than its diff:
```python
import functools
import math

import jax
import jax.numpy as jnp
from jax import lax
from jax.experimental import pallas as pl
from jax.experimental.pallas import tpu as pltpu
from jax.sharding import PartitionSpec as P

epsilon = 1e-06
vmem_share = 2**24


def padded_2(value, sides, width):
    for axis, dim in sides:
        size, length = (lax.axis_size(axis), value.shape[dim])
        up = [(i, (i + 1) % size) for i in range(size - 1)]
        down = [(j, i) for i, j in up]
        last = lax.slice_in_dim(value, length - width, length, axis=dim)
        leading = lax.slice_in_dim(value, 0, width, axis=dim)
        before = lax.ppermute(last, axis, up)
        after = lax.ppermute(leading, axis, down)
        value = jnp.concatenate([before, value, after], axis=dim)
    return value


def normalize(row_values, gain):
    values = row_values.astype(jnp.float32)
    scaled = values * lax.rsqrt(jnp.mean(values * values, axis=-1, keepdims=True) + epsilon)
    return (scaled * gain).astype(jnp.bfloat16)


def pool_groups(padded, start_row, row_count, seq_length):
    group_width = padded.shape[1] // 4
    position = start_row + jnp.arange(row_count, dtype=jnp.int32)
    centre = padded[8 : 8 + row_count]
    pooled_parts = []
    for group_index in range(4):
        window = 2 ** (group_index + 1)
        reach_left = window // 2
        reach_right = window - 1 - reach_left
        group_cols = padded[:, group_index * group_width : (group_index + 1) * group_width]
        window_sum = group_cols[8 - reach_left : 8 - reach_left + row_count]
        for offset in range(1 - reach_left, reach_right + 1):
            window_sum = window_sum + group_cols[8 + offset : 8 + offset + row_count]
        cover = (
            jnp.minimum(position + reach_right + 1, seq_length)
            - jnp.maximum(position - reach_left, 0)
        ).astype(jnp.float32)
        pooled_parts.append(
            window_sum / cover[:, None]
            - centre[:, group_index * group_width : (group_index + 1) * group_width]
        )
    return jnp.stack(pooled_parts, axis=1).astype(jnp.bfloat16)


def mixer(mixer_input, mixer_gain, group_weight, mixer_scale):
    row_count = mixer_input.shape[0]
    normed = normalize(mixer_input, mixer_gain)
    padded = padded_2(normed, ((("ep", "tp"), 0),), 8)
    start_row = lax.axis_index(("ep", "tp")) * row_count
    seq_length = row_count * lax.axis_size(("ep", "tp"))
    pooled = pool_groups(padded.astype(jnp.float32), start_row, row_count, seq_length)
    mixed_groups = jnp.einsum(
        "tgi,gio->tgo", pooled, group_weight, preferred_element_type=jnp.float32
    )
    return (mixed_groups.reshape(row_count, -1) * mixer_scale).astype(jnp.bfloat16)


def routed_plan(expert_input, expert_gain, routes, route_weight, w_gate, w_up, w_down):
    row_count = expert_input.shape[0]
    top_count = routes.shape[1]
    experts = lax.axis_size("ep") * w_gate.shape[0]
    capacity = 3 * top_count * row_count // (2 * experts)
    normed = normalize(expert_input, expert_gain)
    flat_route = routes.reshape(-1)
    onehot = (flat_route[:, None] == jnp.arange(experts, dtype=jnp.int32)[None, :]).astype(
        jnp.int32
    )
    before = jnp.cumsum(onehot, axis=0) - onehot
    slot_index = flat_route * capacity + jnp.sum(before * onehot, axis=1)
    places = (
        slot_index.reshape(row_count, top_count)[None, :, :]
        == jnp.arange(experts * capacity, dtype=jnp.int32)[:, None, None]
    )
    dispatch = jnp.any(places, axis=2).astype(jnp.bfloat16)
    outgoing = jnp.dot(dispatch, normed, preferred_element_type=jnp.float32).astype(jnp.bfloat16)
    arrived = lax.all_to_all(outgoing, "ep", split_axis=0, concat_axis=0, tiled=True)
    down_w = w_down[0]
    paired = jnp.stack((w_gate[0], w_up[0]), axis=0)
    portion = lax.all_gather(paired, "tp", axis=2, tiled=True)
    gate_part = jnp.dot(arrived, portion[0], preferred_element_type=jnp.float32)
    up_part = jnp.dot(arrived, portion[1], preferred_element_type=jnp.float32)
    hidden = (jax.nn.silu(gate_part) * up_part).astype(jnp.bfloat16)
    block_width = down_w.shape[0]
    portion = lax.all_gather(down_w, "tp", axis=0, tiled=True)
    blocks = portion.shape[0] // block_width
    hidden_part = hidden
    hidden_part = hidden_part.reshape(hidden_part.shape[0], blocks, block_width)
    block_terms = jnp.einsum(
        "rkf,kfd->krd",
        hidden_part,
        portion.reshape(blocks, block_width, portion.shape[1]),
        preferred_element_type=jnp.float32,
    )
    rounded = lax.optimization_barrier(block_terms.astype(jnp.bfloat16)).astype(jnp.float32)
    result = jnp.sum(rounded, axis=0)
    returned = lax.all_to_all(
        result.astype(jnp.bfloat16), "ep", split_axis=0, concat_axis=0, tiled=True
    )
    picked = (
        jnp.take(returned, slot_index, axis=0).astype(jnp.float32).reshape(row_count, top_count, -1)
    )
    expert_out = jnp.sum(picked * route_weight[:, :, None], axis=1).astype(jnp.bfloat16)
    return expert_out


def slots(routes, route_weight, experts):
    chosen = routes[:, :, None] == jnp.arange(experts, dtype=jnp.int32)[None, None, :]
    named = jnp.any(chosen, axis=1)
    weight = jnp.sum(jnp.where(chosen, route_weight[:, :, None], 0.0), axis=1)
    rows = routes.shape[0]
    earlier = jnp.arange(rows)[None, :] < jnp.arange(rows)[:, None]
    place = jnp.dot(
        earlier.astype(jnp.bfloat16), named.astype(jnp.bfloat16), preferred_element_type=jnp.float32
    )
    place = jnp.where(named, place, -1.0)
    high = lax.reduce_precision(weight, 8, 7)
    return jnp.concatenate([place, high, weight - high], axis=1).T.astype(jnp.bfloat16)


def near_first(length):
    return [sorted(range(length), key=lambda other: abs(other - at)) for at in range(length)]


def stream_kernel(
    depth, capacity, experts,
    token_ref, gate_ref, up_ref, down_ref, out_ref,
    tok, blk, part, from_core, out_right, out_left, out_far, relay_right, relay_left,
    from_right, from_left, local, dense, dense_above, dense_below,
    far_above, far_below, home_left, home_right, far_back,
    send_sem, recv_sem, local_sem,
):
    column, line = lax.axis_index("ep"), lax.axis_index("tp")
    level, core = line // 2, line % 2
    other = 1 - core
    tall = token_ref.shape[0]
    rows = out_ref.shape[0]
    low = -(-capacity // 32) * 16
    high = capacity - low
    piece = math.gcd(rows, capacity)
    right_column, left_column, far_column = (2 * column + 1) % 5, (3 * column + 2) % 5, 3 - column
    right, left = (right_column, line), (left_column, line)
    beside = (column, level * 2 + other)
    above, below = (column, line + 2), (column, line - 2)
    has_above, has_below = level < depth - 1, level > 0
    f32, bf16 = jnp.float32, jnp.bfloat16

    def level_of(step):
        value = 0
        for at, order in enumerate(near_first(depth)):
            for turn, there in enumerate(order):
                value = value + there * jnp.where((level == at) & (step == turn), 1, 0)
        return value

    def link(src, dst, kind, at, target):
        return pltpu.make_async_remote_copy(
            src_ref=src, dst_ref=dst, send_sem=send_sem.at[kind, at],
            recv_sem=recv_sem.at[kind, at], device_id=target,
            device_id_type=pl.DeviceIdType.MESH,
        )

    def up(at):
        return link(tok.at[at], tok.at[at], 0, at, above)

    def down(at):
        return link(tok.at[at], tok.at[at], 1, at, below)

    def to_right(at):
        return link(out_right.at[at], blk.at[at, 1, core], 2, at, right)

    def to_left(at):
        return link(out_left.at[at], blk.at[at, 2, core], 3, at, left)

    def far_right():
        return link(out_far.at[pl.ds(0, low)], relay_right, 4, 0, right)

    def far_left():
        return link(out_far.at[pl.ds(low, high)], relay_left, 5, 0, left)

    def on_right():
        return link(relay_right, blk.at[level, 3, core, pl.ds(0, low)], 6, 0, right)

    def on_left():
        return link(relay_left, blk.at[level, 3, core, pl.ds(low, high)], 7, 0, left)

    def far_up(at):
        return link(blk.at[at, 3, core], blk.at[at, 3, core], 8, at, above)

    def far_down(at):
        return link(blk.at[at, 3, core], blk.at[at, 3, core], 9, at, below)

    def share(at, q):
        return link(blk.at[at, q, core], blk.at[at, q, core], 10 + q, at, beside)

    def shared_in(at, q):
        return link(blk.at[at, q, other], blk.at[at, q, other], 10 + q, at, beside)

    def give(at, q):
        return link(part.at[at, q, other], from_core.at[at, q], 14 + q, at, beside)

    def back_left(at):
        return link(part.at[at, 1, core], from_right.at[at], 18, at, left)

    def back_right(at):
        return link(part.at[at, 2, core], from_left.at[at], 19, at, right)

    def sum_down(at):
        return link(dense.at[at], dense_above.at[at], 20, at, below)

    def sum_up(at):
        return link(dense.at[at], dense_below.at[at], 21, at, above)

    def far_sum_down(at):
        return link(part.at[at, 3, core], far_above.at[at], 22, at, below)

    def far_sum_up(at):
        return link(part.at[at, 3, core], far_below.at[at], 23, at, above)

    def home_low():
        return link(part.at[level, 3, core, pl.ds(0, low)], home_left, 24, 0, left)

    def home_high():
        return link(part.at[level, 3, core, pl.ds(low, high)], home_right, 25, 0, right)

    def last_low():
        return link(home_left, far_back.at[pl.ds(0, low)], 26, 0, left)

    def last_high():
        return link(home_right, far_back.at[pl.ds(low, high)], 27, 0, right)

    barrier = pltpu.get_barrier_semaphore()

    def greet(target):
        pl.semaphore_signal(
            barrier, inc=1, device_id=target, device_id_type=pl.DeviceIdType.MESH
        )

    greet(right)
    greet(left)
    greet(beside)
    pl.when(has_above)(lambda: greet(above))
    pl.when(has_below)(lambda: greet(below))
    own_copy = pltpu.make_async_copy(token_ref, tok.at[level], local_sem)
    own_copy.start()
    own_copy.wait()
    pl.semaphore_wait(barrier, 3 + jnp.where(has_above, 1, 0) + jnp.where(has_below, 1, 0))

    def table(at):
        listed = tok[at, pl.ds(rows, tall - rows), pl.ds(0, rows)].astype(f32)
        listing = lax.broadcasted_iota(jnp.int32, listed.shape, 0)
        index = lax.broadcasted_iota(jnp.int32, (capacity, rows), 0).astype(f32)

        def row_of(at_row):
            return jnp.sum(jnp.where(listing == at_row, listed, 0.0), axis=0, keepdims=True)

        def hits(expert):
            return index == row_of(expert)

        return row_of, hits

    def picked(at, chosen):
        _, hits = table(at)
        picks = [jnp.where(hits(expert), 1.0, 0.0).astype(bf16) for expert in chosen]
        return jnp.dot(
            jnp.concatenate(picks, axis=0), tok[at, pl.ds(0, rows)], preferred_element_type=f32
        ).astype(bf16)

    def placed(at, chosen, results):
        row_of, hits = table(at)
        total = None
        for kind in (1, 2):
            weights = [
                jnp.where(hits(expert), row_of(kind * experts + expert), 0.0).astype(bf16)
                for expert in chosen
            ]
            term = lax.dot_general(
                jnp.concatenate(weights, axis=0), results,
                (((0,), (0,)), ((), ())), preferred_element_type=f32,
            )
            total = term if total is None else total + term
        return total

    def compute(at, q):
        gathered = jnp.concatenate([blk[at, q, 0], blk[at, q, 1]], axis=0)
        gate_part = jnp.dot(gathered, gate_ref[...], preferred_element_type=f32)
        up_part = jnp.dot(gathered, up_ref[...], preferred_element_type=f32)
        hidden = (gate_part / (1.0 + jnp.exp(-gate_part)) * up_part).astype(bf16)
        partial = jnp.dot(hidden, down_ref[...], preferred_element_type=f32).astype(bf16)
        for lane in range(2):
            part[at, q, lane] = partial[lane * capacity : (lane + 1) * capacity]

    def by_piece(count, body):
        def one(i, carry):
            body(pl.ds(pl.multiple_of(i * piece, piece), piece))
            return carry

        lax.fori_loop(0, count // piece, one, 0)

    def paired(at, q):
        give(at, q).wait_recv()

        def body(span):
            total = part[at, q, core, span].astype(f32) + from_core[at, q, span].astype(f32)
            part[at, q, core, span] = total.astype(bf16)

        by_piece(capacity, body)

    def with_incoming(above_too, below_too, action):
        both = above_too & below_too
        pl.when(both)(lambda: action(True, True))
        pl.when(above_too & jnp.logical_not(both))(lambda: action(True, False))
        pl.when(below_too & jnp.logical_not(both))(lambda: action(False, True))
        pl.when(jnp.logical_not(above_too | below_too))(lambda: action(False, False))

    def far_total(at):
        give(at, 3).wait_recv()
        above_too, below_too = (at <= level) & has_above, (at >= level) & has_below
        pl.when(above_too)(lambda: far_sum_down(at).wait_recv())
        pl.when(below_too)(lambda: far_sum_up(at).wait_recv())

        def action(from_up, from_down):
            def body(span):
                total = part[at, 3, core, span].astype(f32) + from_core[at, 3, span].astype(f32)
                if from_up:
                    total = total + far_above[at, span].astype(f32)
                if from_down:
                    total = total + far_below[at, span].astype(f32)
                part[at, 3, core, span] = total.astype(bf16)

            by_piece(capacity, body)

        with_incoming(above_too, below_too, action)

    def dense_total(at):
        above_too, below_too = (at <= level) & has_above, (at >= level) & has_below
        pl.when(above_too)(lambda: sum_down(at).wait_recv())
        pl.when(below_too)(lambda: sum_up(at).wait_recv())

        def action(from_up, from_down):
            def body(span):
                total = local[at, span]
                if from_up:
                    total = total + dense_above[at, span].astype(f32)
                if from_down:
                    total = total + dense_below[at, span].astype(f32)
                dense[at, span] = total.astype(bf16)

            by_piece(rows, body)

        with_incoming(above_too, below_too, action)

    def expand(at):
        give(at, 0).wait_recv()
        back_left(at).wait_recv()
        back_right(at).wait_recv()
        own = (part[at, 0, core].astype(f32) + from_core[at, 0].astype(f32)).astype(bf16)
        results = jnp.concatenate([own, from_right[at], from_left[at]], axis=0)
        local[at] = placed(at, (column, right_column, left_column), results)

    def arrive(turn):
        at = level_of(turn)
        pl.when(at < level)(lambda: up(at).wait_recv())
        pl.when(at > level)(lambda: down(at).wait_recv())
        pl.when((at <= level) & has_above)(lambda: up(at).start())
        pl.when((at >= level) & has_below)(lambda: down(at).start())

        @pl.when(at == level)
        def _():
            out_far[...] = picked(at, (far_column,))
            far_right().start()
            far_left().start()

        sent = picked(at, (right_column, left_column, column))
        out_right[at] = sent[:capacity]
        out_left[at] = sent[capacity : 2 * capacity]
        to_right(at).start()
        to_left(at).start()
        blk[at, 0, core] = sent[2 * capacity :]
        share(at, 0).start()

    def sides_in(at):
        to_right(at).wait_recv()
        share(at, 1).start()
        to_left(at).wait_recv()
        share(at, 2).start()

    def far_in(at):
        @pl.when(at == level)
        def _():
            on_right().wait_recv()
            on_left().wait_recv()

        pl.when(at < level)(lambda: far_up(at).wait_recv())
        pl.when(at > level)(lambda: far_down(at).wait_recv())
        pl.when((at <= level) & has_above)(lambda: far_up(at).start())
        pl.when((at >= level) & has_below)(lambda: far_down(at).start())
        share(at, 3).start()

    def relay():
        far_right().wait_recv()
        on_right().start()
        far_left().wait_recv()
        on_left().start()

    def stage(turn, carry):
        pl.when(turn < depth)(lambda: arrive(turn))

        def one(q, inner):
            step = turn - jnp.where(q > 0, 1, 0)

            @pl.when((step >= 0) & (step < depth))
            def _():
                at = level_of(step)
                pl.when(q == 1)(lambda: sides_in(at))
                pl.when(q == 3)(lambda: far_in(at))
                shared_in(at, q).wait_recv()
                compute(at, q)
                give(at, q).start()

                @pl.when(q == 2)
                def _():
                    paired(at, 1)
                    back_left(at).start()

                @pl.when(q == 3)
                def _():
                    paired(at, 2)
                    back_right(at).start()

            pl.when((q == 0) & (turn == 0))(relay)
            return inner

        lax.fori_loop(0, 4, one, 0)
        pl.when((turn >= 3) & (turn < depth + 2))(lambda: expand(level_of(turn - 2)))

        def chain(at, inner):
            climb = jnp.where(
                at < level, 2 * (depth - 1) - at - level, at + level
            ) + 2

            @pl.when((at != level) & (turn == climb))
            def _():
                far_total(at)
                pl.when(at < level)(lambda: far_sum_down(at).start())
                pl.when(at > level)(lambda: far_sum_up(at).start())
                dense_total(at)
                pl.when(at < level)(lambda: sum_down(at).start())
                pl.when(at > level)(lambda: sum_up(at).start())

            return inner

        lax.fori_loop(0, depth, chain, 0)
        return carry

    lax.fori_loop(0, 2 * depth, stage, 0)

    far_total(level)
    home_low().start()
    home_high().start()
    expand(level)
    dense_total(level)
    home_low().wait_recv()
    last_low().start()
    home_high().wait_recv()
    last_high().start()
    last_low().wait_recv()
    last_high().wait_recv()
    total = placed(level, (far_column,), far_back[...])
    out_ref[...] = (dense[level].astype(f32) + total).astype(bf16)

    def drain(at, carry):
        upward, downward = (at <= level) & has_above, (at >= level) & has_below
        for copy in (up, far_up):
            pl.when(upward)(lambda copy=copy: copy(at).wait_send())
        for copy in (down, far_down):
            pl.when(downward)(lambda copy=copy: copy(at).wait_send())
        for copy in (to_right, to_left, back_left, back_right):
            copy(at).wait_send()
        for q in range(4):
            share(at, q).wait_send()
            give(at, q).wait_send()
        for copy in (sum_down, far_sum_down):
            pl.when(at < level)(lambda copy=copy: copy(at).wait_send())
        for copy in (sum_up, far_sum_up):
            pl.when(at > level)(lambda copy=copy: copy(at).wait_send())
        return carry

    lax.fori_loop(0, depth, drain, 0)
    for copy in (
        far_right, far_left, on_right, on_left, home_low, home_high, last_low, last_high
    ):
        copy().wait_send()


def dense_plan(expert_input, expert_gain, routes, route_weight, w_gate, w_up, w_down):
    row_count, width = expert_input.shape
    experts = lax.axis_size("ep")
    depth = lax.axis_size("tp") // 2
    capacity = 3 * routes.shape[1] * row_count // (2 * experts)
    normed = normalize(expert_input, expert_gain)
    listed = slots(routes, route_weight, experts)
    pad = -(-3 * experts // 16) * 16
    listed = jnp.pad(listed, ((0, pad - 3 * experts), (0, width - row_count)))
    sent = jnp.concatenate([normed, listed], axis=0)
    bf16 = jnp.bfloat16
    low = -(-capacity // 32) * 16
    high = capacity - low
    vmem = pl.BlockSpec(memory_space=pltpu.VMEM)
    compact = pltpu.VMEM((depth, capacity, width), bf16)
    dense = pltpu.VMEM((depth, row_count, width), bf16)
    return pl.pallas_call(
        functools.partial(stream_kernel, depth, capacity, experts),
        out_shape=jax.ShapeDtypeStruct((row_count, width), bf16),
        in_specs=[vmem] * 4,
        out_specs=vmem,
        scratch_shapes=[
            pltpu.VMEM((depth, row_count + pad, width), bf16),
            pltpu.VMEM((depth, 4, 2, capacity, width), bf16),
            pltpu.VMEM((depth, 4, 2, capacity, width), bf16),
            pltpu.VMEM((depth, 4, capacity, width), bf16),
            compact,
            compact,
            pltpu.VMEM((capacity, width), bf16),
            pltpu.VMEM((low, width), bf16),
            pltpu.VMEM((high, width), bf16),
            compact,
            compact,
            pltpu.VMEM((depth, row_count, width), jnp.float32),
            dense,
            dense,
            dense,
            compact,
            compact,
            pltpu.VMEM((low, width), bf16),
            pltpu.VMEM((high, width), bf16),
            pltpu.VMEM((capacity, width), bf16),
            pltpu.SemaphoreType.DMA((28, depth)),
            pltpu.SemaphoreType.DMA((28, depth)),
            pltpu.SemaphoreType.DMA,
        ],
        compiler_params=pltpu.CompilerParams(
            collective_id=0, has_side_effects=True, vmem_limit_bytes=60 * 2**20
        ),
    )(sent, w_gate[0], w_up[0], w_down[0])


def on_device(
    mixer_input, mixer_gain, group_weight, mixer_scale,
    expert_input, expert_gain, routes, route_weight, w_gate, w_up, w_down,
):
    devices = lax.axis_size(("ep", "tp"))
    gathered_bytes = 2 * devices * expert_input.size
    square = lax.axis_size("ep") == 4
    plan = dense_plan if square and gathered_bytes <= vmem_share else routed_plan
    expert_out = plan(expert_input, expert_gain, routes, route_weight, w_gate, w_up, w_down)
    return (mixer(mixer_input, mixer_gain, group_weight, mixer_scale), expert_out)


def solution(mesh):
    placed = (
        P(("ep", "tp"), None),
        P(),
        P(),
        P(),
        P(("ep", "tp"), None),
        P(),
        P(("ep", "tp"), None),
        P(("ep", "tp"), None),
        P("ep", None, "tp"),
        P("ep", None, "tp"),
        P("ep", "tp", None),
    )
    return jax.shard_map(
        on_device,
        mesh=mesh,
        in_specs=placed,
        out_specs=(P(("ep", "tp"), None), P(("ep", "tp"), None)),
        check_vma=False,
    )
```

time: 143 us -> 152 us (1.063)
  Pallas kernels: 130 us -> 139 us
    pallas_call x1, Pallas kernels: 130 us -> 139 us  [dense_plan(): pl.pallas_call(functools.partial(stream_kernel, depth, capacity, experts)...]
where the time goes in v1:
time: 152 us
  Pallas kernels  139 us (91%)
  other arithmetic  4.74 us (3%)
  starting transfers between devices  3.69 us (2%)
  local copies, waits for them, and re-layouts  3.54 us (2%)
    pallas_call x1, Pallas kernels, dense_plan(): pl.pallas_call(functools.partial(stream_kernel, depth, capacity, experts)...  139 us
    unnamed x17, local copies, waits for them, and re-layouts  3.46 us
  transfers between devices with their start and end apart: 2, of which 0 were waited for; matrix products, arithmetic and copies ran while one was open for 1% of the time, Pallas kernels for 91%

profile of v1, /device:TPU:0, one launch (start us, length us, event | category | flops | bytes accessed | tf_op | source)
XLA Modules:
  0.0 151.9 jit_solution(13867664880644917493)
XLA Ops:
  0.6 0.0 copy-start
  0.6 0.0 copy-start.1
  0.7 1.2 fusion.2
  1.9 0.0 copy-done.1
  1.9 0.0 copy-start.2
  1.9 0.9 fusion.4
  2.8 2.4 %collective-permute-start = (bf16[8,1024]{1,0:T(8,128)(2,1)S(1)}, bf16[8,1024]{1,0:T(8,128)(2,1)S(1)}, u32[]{:S(2)}, u32[]{:S(2)}) collective-permute-start(bf16[8,1024]{1,0:T(8,128)(2,1)S(1)} %get-tuple-element.5), channel_id=1, source_target_pairs={{0,1},{1,2},{2,3},{3,4},{4,5},{5,6},{6,7},{7,8},{8,9},{9,10},{10,1... | collective-permute-start | bytes 49160 | tf_op jit(solution)/shard_map/ppermute | solution.py:22
  5.2 1.3 collective-permute-start.1
  6.5 0.0 copy-start.4
  6.6 0.7 copy-done.4
  7.2 0.0 copy-start.7
  7.2 0.7 copy-done.7
  7.9 0.1 fusion
  8.1 0.0 copy-done.2
  8.1 0.2 fusion.5
  8.3 0.5 copy-done.5
  8.8 0.2 fusion.7
  9.0 0.8 fusion.8.token_ref
  9.8 138.7 %shard_map.122 = bf16[192,1024]{1,0:T(8,128)(2,1)} custom-call(bf16[208,1024]{1,0:T(8,128)(2,1)} %fusion.8.token_ref, bf16[1024,512]{1,0:T(8,128)(2,1)} %bitcast.20, bf16[1024,512]{1,0:T(8,128)(2,1)} %bitcast.21, bf16[512,1024]{1,0:T(8,128)(2,1)} %bitcast.22), custom_call_target="tpu_custom_call" | custom-call | tf_op jit(solution)/shard_map/pallas_call | solution.py:523
  148.5 0.0 collective-permute-done
  148.5 0.0 collective-permute-done.1
  148.5 0.1 maximum_convert_fusion
  148.6 0.2 fusion.34
  148.8 0.3 fusion.31
  149.1 0.0 copy-done
  149.1 0.3 convolution_bitcast_fusion
  149.4 0.0 copy-start.6
  149.4 0.1 copy.19
  149.5 0.6 copy-done.6
  150.1 0.8 multiply_convert_fusion
  150.9 0.2 copy-done.3
  151.1 0.7 copy.21
  (11 shorter events, 0.1 us)
Async XLA Ops:
  0.6 148.5 %copy-start = (bf16[4,256,256]{2,1,0:T(8,128)(2,1)S(1)}, bf16[4,256,256]{2,1,0:T(8,128)(2,1)}, u32[]{:S(2)}) copy-start(bf16[4,256,256]{2,1,0:T(8,128)(2,1)} %param.13) | copy-start | bytes 1572868
  0.6 1.3 copy-start.1
  1.9 6.2 %copy-start.2 = (bf16[192,1024]{1,0:T(8,128)(2,1)S(1)}, bf16[192,1024]{1,0:T(8,128)(2,1)}, u32[]{:S(2)}) copy-start(bf16[192,1024]{1,0:T(8,128)(2,1)} %param.15) | copy-start | bytes 1179652
  2.8 145.6 %collective-permute-start = (bf16[8,1024]{1,0:T(8,128)(2,1)S(1)}, bf16[8,1024]{1,0:T(8,128)(2,1)S(1)}, u32[]{:S(2)}, u32[]{:S(2)}) collective-permute-start(bf16[8,1024]{1,0:T(8,128)(2,1)S(1)} %get-tuple-element.5), channel_id=1, source_target_pairs={{0,1},{1,2},{2,3},{3,4},{4,5},{5,6},{6,7},{7,8},{8,9},{9,10},{10,1... | collective-permute-start | bytes 49160 | tf_op jit(solution)/shard_map/ppermute | solution.py:22
  5.2 143.2 %collective-permute-start.1 = (bf16[8,1024]{1,0:T(8,128)(2,1)S(1)}, bf16[8,1024]{1,0:T(8,128)(2,1)S(1)}, u32[]{:S(2)}, u32[]{:S(2)}) collective-permute-start(bf16[8,1024]{1,0:T(8,128)(2,1)S(1)} %get-tuple-element.6), channel_id=1, source_target_pairs={{1,0},{2,1},{3,2},{4,3},{5,4},{6,5},{7,6},{8,7},{9,8},{10,9},{11,1... | collective-permute-start | bytes 49160 | tf_op jit(solution)/shard_map/ppermute | solution.py:23
  6.5 0.7 copy-start.4
  7.2 0.7 copy-start.7
  8.1 0.7 copy-start.5
  149.4 0.7 copy-start.6
  150.1 1.1 copy-start.3

commit v2 on v1

--- a/solution.py
+++ b/solution.py
@@ -130,14 +130,55 @@
     return jnp.concatenate([place, high, weight - high], axis=1).T.astype(jnp.bfloat16)
 
 
-def near_first(length):
-    return [sorted(range(length), key=lambda other: abs(other - at)) for at in range(length)]
+ORDERS = (
+    (
+        ("D", 0, 1), ("D", 0, 0), ("X", 0, 0), ("Y", 0, 0), ("M", 0, 0), ("D", 1, 0), ("G", 0, 0),
+        ("D", 1, 1), ("M", 1, 0), ("D", 2, 1), ("D", 2, 0), ("C", 0, 0), ("M", 2, 0), ("C", 2, 0),
+        ("I", 0, 0), ("C", 0, 2), ("C", 0, 1), ("D", 3, 1), ("D", 3, 0), ("M", 3, 0), ("I", 2, 0),
+        ("G", 1, 0), ("P", 0, 1), ("C", 2, 2), ("C", 1, 3), ("C", 2, 1), ("I", 3, 0), ("F", 1, 0),
+        ("I", 1, 0), ("G", 2, 0), ("C", 3, 2), ("F", 1, 1), ("C", 2, 3), ("C", 3, 1), ("F", 2, 0),
+        ("P", 3, 2), ("C", 1, 2), ("P", 2, 2), ("P", 3, 1), ("P", 2, 1), ("F", 2, 1), ("G", 3, 0),
+        ("C", 3, 3), ("C", 1, 0), ("F", 3, 0), ("F", 3, 1), ("C", 3, 0), ("C", 0, 3), ("C", 1, 1),
+        ("E", 3, 0), ("P", 1, 2), ("P", 1, 1), ("P", 0, 2), ("S", 3, 0), ("S", 3, 1), ("E", 2, 0),
+        ("S", 2, 0), ("S", 2, 1), ("F", 0, 0), ("E", 1, 0), ("S", 1, 0), ("F", 0, 1), ("V", 0, 0),
+        ("V", 0, 1), ("E", 0, 0), ("S", 1, 1), ("S", 0, 0), ("S", 0, 1), ("Z", 0, 0),
+    ),
+    (
+        ("D", 1, 0), ("D", 1, 1), ("X", 1, 0), ("M", 1, 0), ("Y", 1, 0), ("D", 2, 0), ("D", 0, 0),
+        ("D", 2, 1), ("I", 1, 0), ("D", 0, 1), ("M", 0, 0), ("D", 3, 0), ("C", 1, 1), ("D", 3, 1),
+        ("M", 3, 0), ("I", 0, 0), ("G", 1, 0), ("C", 0, 1), ("P", 0, 1), ("C", 1, 3), ("G", 0, 0),
+        ("I", 3, 0), ("G", 2, 0), ("C", 0, 3), ("C", 3, 2), ("M", 2, 0), ("C", 3, 1), ("P", 3, 2),
+        ("C", 0, 2), ("G", 3, 0), ("P", 3, 1), ("C", 1, 2), ("C", 2, 0), ("C", 1, 0), ("C", 3, 3),
+        ("I", 2, 0), ("C", 2, 3), ("P", 0, 2), ("P", 1, 1), ("C", 2, 2), ("C", 2, 1), ("C", 0, 0),
+        ("P", 1, 2), ("F", 2, 0), ("F", 2, 1), ("C", 3, 0), ("F", 3, 0), ("F", 1, 0), ("P", 2, 2),
+        ("F", 3, 1), ("P", 2, 1), ("F", 0, 0), ("E", 3, 0), ("S", 3, 0), ("E", 1, 0), ("E", 0, 0),
+        ("F", 1, 1), ("V", 1, 0), ("F", 0, 1), ("S", 3, 1), ("E", 2, 0), ("S", 0, 0), ("S", 2, 0),
+        ("S", 0, 1), ("S", 2, 1), ("V", 1, 1), ("S", 1, 0), ("S", 1, 1), ("Z", 1, 0),
+    ),
+)
+
+
+def coded_orders(depth, kinds):
+    base = len(kinds) * 4 * depth + 1
+    per_word = 1
+    while base ** (per_word + 1) < 2**31:
+        per_word += 1
+    idle = base - 1
+    words = []
+    for order in ORDERS:
+        codes = [(kinds.index(kind) * depth + at) * 4 + q for kind, at, q in order]
+        codes += [idle] * (-len(codes) % per_word)
+        words.append([
+            sum(code * base**n for n, code in enumerate(codes[first : first + per_word]))
+            for first in range(0, len(codes), per_word)
+        ])
+    return words, per_word, base
 
 
 def stream_kernel(
     depth, capacity, experts,
-    token_ref, gate_ref, up_ref, down_ref, out_ref,
-    tok, blk, part, from_core, out_right, out_left, out_far, relay_right, relay_left,
+    token_ref, table_ref, gate_ref, up_ref, down_ref, out_ref,
+    tok, tables, blk, part, from_core, out_right, out_left, out_far, relay_right, relay_left,
     from_right, from_left, local, dense, dense_above, dense_below,
     far_above, far_below, home_left, home_right, far_back,
     send_sem, recv_sem, local_sem,
@@ -145,11 +186,12 @@
     column, line = lax.axis_index("ep"), lax.axis_index("tp")
     level, core = line // 2, line % 2
     other = 1 - core
-    tall = token_ref.shape[0]
     rows = out_ref.shape[0]
+    half = rows // 2
     low = -(-capacity // 32) * 16
     high = capacity - low
-    piece = math.gcd(rows, capacity)
+    piece = math.gcd(half, capacity)
+    step_rows = math.gcd(low, high)
     right_column, left_column, far_column = (2 * column + 1) % 5, (3 * column + 2) % 5, 3 - column
     right, left = (right_column, line), (left_column, line)
     beside = (column, level * 2 + other)
@@ -157,13 +199,6 @@
     has_above, has_below = level < depth - 1, level > 0
     f32, bf16 = jnp.float32, jnp.bfloat16
 
-    def level_of(step):
-        value = 0
-        for at, order in enumerate(near_first(depth)):
-            for turn, there in enumerate(order):
-                value = value + there * jnp.where((level == at) & (step == turn), 1, 0)
-        return value
-
     def link(src, dst, kind, at, target):
         return pltpu.make_async_remote_copy(
             src_ref=src, dst_ref=dst, send_sem=send_sem.at[kind, at],
@@ -171,74 +206,85 @@
             device_id_type=pl.DeviceIdType.MESH,
         )
 
-    def up(at):
-        return link(tok.at[at], tok.at[at], 0, at, above)
-
-    def down(at):
-        return link(tok.at[at], tok.at[at], 1, at, below)
+    def part_of(h):
+        return pl.ds(pl.multiple_of(h * half, half), half)
+
+    def up(at, h):
+        return link(tok.at[at, part_of(h)], tok.at[at, part_of(h)], h, at, above)
+
+    def down(at, h):
+        return link(tok.at[at, part_of(h)], tok.at[at, part_of(h)], 2 + h, at, below)
+
+    def table_up(at):
+        return link(tables.at[at], tables.at[at], 4, at, above)
+
+    def table_down(at):
+        return link(tables.at[at], tables.at[at], 5, at, below)
 
     def to_right(at):
-        return link(out_right.at[at], blk.at[at, 1, core], 2, at, right)
+        return link(out_right.at[at], blk.at[at, 1, core], 6, at, right)
 
     def to_left(at):
-        return link(out_left.at[at], blk.at[at, 2, core], 3, at, left)
+        return link(out_left.at[at], blk.at[at, 2, core], 7, at, left)
 
     def far_right():
-        return link(out_far.at[pl.ds(0, low)], relay_right, 4, 0, right)
+        return link(out_far.at[pl.ds(0, low)], relay_right, 8, 0, right)
 
     def far_left():
-        return link(out_far.at[pl.ds(low, high)], relay_left, 5, 0, left)
+        return link(out_far.at[pl.ds(low, high)], relay_left, 9, 0, left)
 
     def on_right():
-        return link(relay_right, blk.at[level, 3, core, pl.ds(0, low)], 6, 0, right)
+        return link(relay_right, blk.at[level, 3, core, pl.ds(0, low)], 10, 0, right)
 
     def on_left():
-        return link(relay_left, blk.at[level, 3, core, pl.ds(low, high)], 7, 0, left)
+        return link(relay_left, blk.at[level, 3, core, pl.ds(low, high)], 11, 0, left)
 
     def far_up(at):
-        return link(blk.at[at, 3, core], blk.at[at, 3, core], 8, at, above)
+        return link(blk.at[at, 3, core], blk.at[at, 3, core], 12, at, above)
 
     def far_down(at):
-        return link(blk.at[at, 3, core], blk.at[at, 3, core], 9, at, below)
+        return link(blk.at[at, 3, core], blk.at[at, 3, core], 13, at, below)
 
     def share(at, q):
-        return link(blk.at[at, q, core], blk.at[at, q, core], 10 + q, at, beside)
+        return link(blk.at[at, q, core], blk.at[at, q, core], 14 + q, at, beside)
 
     def shared_in(at, q):
-        return link(blk.at[at, q, other], blk.at[at, q, other], 10 + q, at, beside)
+        return link(blk.at[at, q, other], blk.at[at, q, other], 14 + q, at, beside)
 
     def give(at, q):
-        return link(part.at[at, q, other], from_core.at[at, q], 14 + q, at, beside)
+        return link(part.at[at, q, other], from_core.at[at, q], 18 + q, at, beside)
 
     def back_left(at):
-        return link(part.at[at, 1, core], from_right.at[at], 18, at, left)
+        return link(part.at[at, 1, core], from_right.at[at], 22, at, left)
 
     def back_right(at):
-        return link(part.at[at, 2, core], from_left.at[at], 19, at, right)
-
-    def sum_down(at):
-        return link(dense.at[at], dense_above.at[at], 20, at, below)
-
-    def sum_up(at):
-        return link(dense.at[at], dense_below.at[at], 21, at, above)
-
-    def far_sum_down(at):
-        return link(part.at[at, 3, core], far_above.at[at], 22, at, below)
-
-    def far_sum_up(at):
-        return link(part.at[at, 3, core], far_below.at[at], 23, at, above)
+        return link(part.at[at, 2, core], from_left.at[at], 23, at, right)
+
+    def sum_down(at, h):
+        return link(dense.at[at, part_of(h)], dense_above.at[at, part_of(h)], 24 + h, at, below)
+
+    def sum_up(at, h):
+        return link(dense.at[at, part_of(h)], dense_below.at[at, part_of(h)], 26 + h, at, above)
+
+    cuts = (pl.ds(0, low), pl.ds(low, high))
+
+    def far_sum_down(at, h):
+        return link(part.at[at, 3, core, cuts[h]], far_above.at[at, cuts[h]], 28 + h, at, below)
+
+    def far_sum_up(at, h):
+        return link(part.at[at, 3, core, cuts[h]], far_below.at[at, cuts[h]], 30 + h, at, above)
 
     def home_low():
-        return link(part.at[level, 3, core, pl.ds(0, low)], home_left, 24, 0, left)
+        return link(part.at[level, 3, core, cuts[0]], home_left, 32, 0, left)
 
     def home_high():
-        return link(part.at[level, 3, core, pl.ds(low, high)], home_right, 25, 0, right)
+        return link(part.at[level, 3, core, cuts[1]], home_right, 33, 0, right)
 
     def last_low():
-        return link(home_left, far_back.at[pl.ds(0, low)], 26, 0, left)
+        return link(home_left, far_back.at[cuts[0]], 34, 0, left)
 
     def last_high():
-        return link(home_right, far_back.at[pl.ds(low, high)], 27, 0, right)
+        return link(home_right, far_back.at[cuts[1]], 35, 0, right)
 
     barrier = pltpu.get_barrier_semaphore()
 
@@ -255,10 +301,13 @@
     own_copy = pltpu.make_async_copy(token_ref, tok.at[level], local_sem)
     own_copy.start()
     own_copy.wait()
+    own_table = pltpu.make_async_copy(table_ref, tables.at[level], local_sem)
+    own_table.start()
+    own_table.wait()
     pl.semaphore_wait(barrier, 3 + jnp.where(has_above, 1, 0) + jnp.where(has_below, 1, 0))
 
     def table(at):
-        listed = tok[at, pl.ds(rows, tall - rows), pl.ds(0, rows)].astype(f32)
+        listed = tables[at, :, pl.ds(0, rows)].astype(f32)
         listing = lax.broadcasted_iota(jnp.int32, listed.shape, 0)
         index = lax.broadcasted_iota(jnp.int32, (capacity, rows), 0).astype(f32)
 
@@ -274,7 +323,7 @@
         _, hits = table(at)
         picks = [jnp.where(hits(expert), 1.0, 0.0).astype(bf16) for expert in chosen]
         return jnp.dot(
-            jnp.concatenate(picks, axis=0), tok[at, pl.ds(0, rows)], preferred_element_type=f32
+            jnp.concatenate(picks, axis=0), tok[at], preferred_element_type=f32
         ).astype(bf16)
 
     def placed(at, chosen, results):
@@ -301,12 +350,12 @@
         for lane in range(2):
             part[at, q, lane] = partial[lane * capacity : (lane + 1) * capacity]
 
-    def by_piece(count, body):
+    def by_piece(start, count, width, body):
         def one(i, carry):
-            body(pl.ds(pl.multiple_of(i * piece, piece), piece))
+            body(pl.ds(pl.multiple_of(start + i * width, width), width))
             return carry
 
-        lax.fori_loop(0, count // piece, one, 0)
+        lax.fori_loop(0, count // width, one, 0)
 
     def paired(at, q):
         give(at, q).wait_recv()
@@ -315,7 +364,7 @@
             total = part[at, q, core, span].astype(f32) + from_core[at, q, span].astype(f32)
             part[at, q, core, span] = total.astype(bf16)
 
-        by_piece(capacity, body)
+        by_piece(0, capacity, piece, body)
 
     def with_incoming(above_too, below_too, action):
         both = above_too & below_too
@@ -324,11 +373,10 @@
         pl.when(below_too & jnp.logical_not(both))(lambda: action(False, True))
         pl.when(jnp.logical_not(above_too | below_too))(lambda: action(False, False))
 
-    def far_total(at):
-        give(at, 3).wait_recv()
+    def far_total(at, h):
         above_too, below_too = (at <= level) & has_above, (at >= level) & has_below
-        pl.when(above_too)(lambda: far_sum_down(at).wait_recv())
-        pl.when(below_too)(lambda: far_sum_up(at).wait_recv())
+        pl.when(above_too)(lambda: far_sum_down(at, h).wait_recv())
+        pl.when(below_too)(lambda: far_sum_up(at, h).wait_recv())
 
         def action(from_up, from_down):
             def body(span):
@@ -339,14 +387,22 @@
                     total = total + far_below[at, span].astype(f32)
                 part[at, 3, core, span] = total.astype(bf16)
 
-            by_piece(capacity, body)
+            by_piece((0, low)[h], (low, high)[h], step_rows, body)
 
         with_incoming(above_too, below_too, action)
-
-    def dense_total(at):
+        pl.when(at < level)(lambda: far_sum_down(at, h).start())
+        pl.when(at > level)(lambda: far_sum_up(at, h).start())
+        pl.when(at == level)(lambda: (home_low, home_high)[h]().start())
+
+    def far_step(at, h):
+        pl.when(h == 0)(lambda: give(at, 3).wait_recv())
+        pl.when(h == 0)(lambda: far_total(at, 0))
+        pl.when(h == 1)(lambda: far_total(at, 1))
+
+    def dense_step(at, h):
         above_too, below_too = (at <= level) & has_above, (at >= level) & has_below
-        pl.when(above_too)(lambda: sum_down(at).wait_recv())
-        pl.when(below_too)(lambda: sum_up(at).wait_recv())
+        pl.when(above_too)(lambda: sum_down(at, h).wait_recv())
+        pl.when(below_too)(lambda: sum_up(at, h).wait_recv())
 
         def action(from_up, from_down):
             def body(span):
@@ -357,11 +413,13 @@
                     total = total + dense_below[at, span].astype(f32)
                 dense[at, span] = total.astype(bf16)
 
-            by_piece(rows, body)
+            by_piece(h * half, half, piece, body)
 
         with_incoming(above_too, below_too, action)
-
-    def expand(at):
+        pl.when(at < level)(lambda: sum_down(at, h).start())
+        pl.when(at > level)(lambda: sum_up(at, h).start())
+
+    def expand(at, _):
         give(at, 0).wait_recv()
         back_left(at).wait_recv()
         back_right(at).wait_recv()
@@ -369,19 +427,33 @@
         results = jnp.concatenate([own, from_right[at], from_left[at]], axis=0)
         local[at] = placed(at, (column, right_column, left_column), results)
 
-    def arrive(turn):
-        at = level_of(turn)
-        pl.when(at < level)(lambda: up(at).wait_recv())
-        pl.when(at > level)(lambda: down(at).wait_recv())
-        pl.when((at <= level) & has_above)(lambda: up(at).start())
-        pl.when((at >= level) & has_below)(lambda: down(at).start())
-
-        @pl.when(at == level)
+    def arrive(at, h):
+        upward, downward = (at <= level) & has_above, (at >= level) & has_below
+
+        @pl.when(h == 0)
         def _():
-            out_far[...] = picked(at, (far_column,))
-            far_right().start()
-            far_left().start()
-
+            pl.when(at < level)(lambda: table_up(at).wait_recv())
+            pl.when(at > level)(lambda: table_down(at).wait_recv())
+            pl.when(upward)(lambda: table_up(at).start())
+            pl.when(downward)(lambda: table_down(at).start())
+
+        pl.when(at < level)(lambda: up(at, h).wait_recv())
+        pl.when(at > level)(lambda: down(at, h).wait_recv())
+        pl.when(upward)(lambda: up(at, h).start())
+        pl.when(downward)(lambda: down(at, h).start())
+
+    def far_out(at, _):
+        out_far[...] = picked(at, (far_column,))
+        far_right().start()
+        far_left().start()
+
+    def relay(at, _):
+        far_right().wait_recv()
+        on_right().start()
+        far_left().wait_recv()
+        on_left().start()
+
+    def sides_out(at, _):
         sent = picked(at, (right_column, left_column, column))
         out_right[at] = sent[:capacity]
         out_left[at] = sent[capacity : 2 * capacity]
@@ -390,13 +462,13 @@
         blk[at, 0, core] = sent[2 * capacity :]
         share(at, 0).start()
 
-    def sides_in(at):
+    def sides_in(at, _):
         to_right(at).wait_recv()
         share(at, 1).start()
         to_left(at).wait_recv()
         share(at, 2).start()
 
-    def far_in(at):
+    def far_in(at, _):
         @pl.when(at == level)
         def _():
             on_right().wait_recv()
@@ -408,93 +480,91 @@
         pl.when((at >= level) & has_below)(lambda: far_down(at).start())
         share(at, 3).start()
 
-    def relay():
-        far_right().wait_recv()
-        on_right().start()
-        far_left().wait_recv()
-        on_left().start()
-
-    def stage(turn, carry):
-        pl.when(turn < depth)(lambda: arrive(turn))
-
-        def one(q, inner):
-            step = turn - jnp.where(q > 0, 1, 0)
-
-            @pl.when((step >= 0) & (step < depth))
-            def _():
-                at = level_of(step)
-                pl.when(q == 1)(lambda: sides_in(at))
-                pl.when(q == 3)(lambda: far_in(at))
-                shared_in(at, q).wait_recv()
-                compute(at, q)
-                give(at, q).start()
-
-                @pl.when(q == 2)
+    def multiply(at, q):
+        shared_in(at, q).wait_recv()
+        compute(at, q)
+        give(at, q).start()
+
+    def back(at, q):
+        paired(at, q)
+        pl.when(q == 1)(lambda: back_left(at).start())
+        pl.when(q == 2)(lambda: back_right(at).start())
+
+    def home_relay(at, h):
+        @pl.when(h == 0)
+        def _():
+            home_low().wait_recv()
+            last_low().start()
+
+        @pl.when(h == 1)
+        def _():
+            home_high().wait_recv()
+            last_high().start()
+
+    def finish(at, _):
+        last_low().wait_recv()
+        last_high().wait_recv()
+        total = placed(level, (far_column,), far_back[...])
+        out_ref[...] = (dense[level].astype(f32) + total).astype(bf16)
+
+    actions = dict(
+        D=arrive, M=sides_out, I=sides_in, G=far_in,
+        C=multiply, P=back, F=far_step, S=dense_step,
+        E=expand, X=far_out, Y=relay, V=home_relay, Z=finish,
+    )
+    kinds = list(actions)
+    words, per_word, base = coded_orders(depth, kinds)
+    mirrored = level >= depth // 2
+    row = jnp.where(mirrored, depth - 1 - level, level)
+
+    def one_word(place, carry):
+        word = 0
+        for at, listing in enumerate(words):
+            for turn, value in enumerate(listing):
+                word = word + jnp.where((row == at) & (place == turn), value, 0)
+
+        def one_step(_, rest):
+            code = rest % base
+            kind, at, q = code // (4 * depth), code // 4 % depth, code % 4
+            at = jnp.where(mirrored, depth - 1 - at, at)
+            for first in range(0, len(kinds), 4):
+
+                @pl.when((kind >= first) & (kind < first + 4))
                 def _():
-                    paired(at, 1)
-                    back_left(at).start()
-
-                @pl.when(q == 3)
-                def _():
-                    paired(at, 2)
-                    back_right(at).start()
-
-            pl.when((q == 0) & (turn == 0))(relay)
-            return inner
-
-        lax.fori_loop(0, 4, one, 0)
-        pl.when((turn >= 3) & (turn < depth + 2))(lambda: expand(level_of(turn - 2)))
-
-        def chain(at, inner):
-            climb = jnp.where(
-                at < level, 2 * (depth - 1) - at - level, at + level
-            ) + 2
-
-            @pl.when((at != level) & (turn == climb))
-            def _():
-                far_total(at)
-                pl.when(at < level)(lambda: far_sum_down(at).start())
-                pl.when(at > level)(lambda: far_sum_up(at).start())
-                dense_total(at)
-                pl.when(at < level)(lambda: sum_down(at).start())
-                pl.when(at > level)(lambda: sum_up(at).start())
-
-            return inner
-
-        lax.fori_loop(0, depth, chain, 0)
+                    for number in range(first, min(first + 4, len(kinds))):
+                        pl.when(kind == number)(
+                            functools.partial(actions[kinds[number]], at, q)
+                        )
+
+            return rest // base
+
+        lax.fori_loop(0, per_word, one_step, word)
         return carry
 
-    lax.fori_loop(0, 2 * depth, stage, 0)
-
-    far_total(level)
-    home_low().start()
-    home_high().start()
-    expand(level)
-    dense_total(level)
-    home_low().wait_recv()
-    last_low().start()
-    home_high().wait_recv()
-    last_high().start()
-    last_low().wait_recv()
-    last_high().wait_recv()
-    total = placed(level, (far_column,), far_back[...])
-    out_ref[...] = (dense[level].astype(f32) + total).astype(bf16)
+    lax.fori_loop(0, len(words[0]), one_word, 0)
 
     def drain(at, carry):
         upward, downward = (at <= level) & has_above, (at >= level) & has_below
-        for copy in (up, far_up):
-            pl.when(upward)(lambda copy=copy: copy(at).wait_send())
-        for copy in (down, far_down):
-            pl.when(downward)(lambda copy=copy: copy(at).wait_send())
+
+        def settle(use, copy, *more):
+            pl.when(use)(lambda: copy(at, *more).wait_send())
+
+        settle(upward, table_up)
+        settle(downward, table_down)
+        settle(upward, far_up)
+        settle(downward, far_down)
+        for h in range(2):
+            settle(upward, up, h)
+            settle(downward, down, h)
+            settle(at < level, sum_down, h)
+            settle(at > level, sum_up, h)
+            settle(at < level, far_sum_down, h)
+            settle(at > level, far_sum_up, h)
         for copy in (to_right, to_left, back_left, back_right):
             copy(at).wait_send()
         for q in range(4):
             share(at, q).wait_send()
             give(at, q).wait_send()
-        for copy in (sum_down, far_sum_down):
-            pl.when(at < level)(lambda copy=copy: copy(at).wait_send())
-        for copy in (sum_up, far_sum_up):
-            pl.when(at > level)(lambda copy=copy: copy(at).wait_send())
         return carry
 
     lax.fori_loop(0, depth, drain, 0)
@@ -512,8 +582,8 @@
     normed = normalize(expert_input, expert_gain)
     listed = slots(routes, route_weight, experts)
     pad = -(-3 * experts // 16) * 16
-    listed = jnp.pad(listed, ((0, pad - 3 * experts), (0, width - row_count)))
-    sent = jnp.concatenate([normed, listed], axis=0)
+    lanes = -(-row_count // 128) * 128
+    listed = jnp.pad(listed, ((0, pad - 3 * experts), (0, lanes - row_count)))
     bf16 = jnp.bfloat16
     low = -(-capacity // 32) * 16
     high = capacity - low
@@ -523,10 +593,11 @@
     return pl.pallas_call(
         functools.partial(stream_kernel, depth, capacity, experts),
         out_shape=jax.ShapeDtypeStruct((row_count, width), bf16),
-        in_specs=[vmem] * 4,
+        in_specs=[vmem] * 5,
         out_specs=vmem,
         scratch_shapes=[
-            pltpu.VMEM((depth, row_count + pad, width), bf16),
+            pltpu.VMEM((depth, row_count, width), bf16),
+            pltpu.VMEM((depth, pad, lanes), bf16),
             pltpu.VMEM((depth, 4, 2, capacity, width), bf16),
             pltpu.VMEM((depth, 4, 2, capacity, width), bf16),
             pltpu.VMEM((depth, 4, capacity, width), bf16),
@@ -546,14 +617,14 @@
             pltpu.VMEM((low, width), bf16),
             pltpu.VMEM((high, width), bf16),
             pltpu.VMEM((capacity, width), bf16),
-            pltpu.SemaphoreType.DMA((28, depth)),
-            pltpu.SemaphoreType.DMA((28, depth)),
+            pltpu.SemaphoreType.DMA((36, depth)),
+            pltpu.SemaphoreType.DMA((36, depth)),
             pltpu.SemaphoreType.DMA,
         ],
         compiler_params=pltpu.CompilerParams(
             collective_id=0, has_side_effects=True, vmem_limit_bytes=60 * 2**20
         ),
-    )(sent, w_gate[0], w_up[0], w_down[0])
+    )(normed, listed, w_gate[0], w_up[0], w_down[0])
 
 
 def on_device(
@@ -562,7 +633,7 @@
 ):
     devices = lax.axis_size(("ep", "tp"))
     gathered_bytes = 2 * devices * expert_input.size
-    square = lax.axis_size("ep") == 4
+    square = lax.axis_size("ep") == 4 and lax.axis_size("tp") == 4 * len(ORDERS)
     plan = dense_plan if square and gathered_bytes <= vmem_share else routed_plan
     expert_out = plan(expert_input, expert_gain, routes, route_weight, w_gate, w_up, w_down)
     return (mixer(mixer_input, mixer_gain, group_weight, mixer_scale), expert_out)

time: 152 us -> 111 us (0.73); the launches traced: 152 us -> 109 us
  Pallas kernels: 139 us -> 95.2 us
    pallas_call x1, Pallas kernels: 139 us -> 95.2 us  [dense_plan(): pl.pallas_call(functools.partial(stream_kernel, depth, capacity, experts)...]
  transfers between devices with their start and end apart: 2 -> 2, of which waited for: 0 -> 0; matrix products, arithmetic and copies ran while one was open for 1% -> 2% of each run, Pallas kernels for 91% -> 87%
where the time goes in v2:
time: 111 us; the launch traced here: 109 us
  Pallas kernels  95.2 us (86%)
  other arithmetic  4.7 us (4%)
  local copies, waits for them, and re-layouts  4.15 us (4%)
  starting transfers between devices  3.69 us (3%)
    pallas_call x1, Pallas kernels, dense_plan(): pl.pallas_call(functools.partial(stream_kernel, depth, capacity, experts)...  95.2 us
    unnamed x17, local copies, waits for them, and re-layouts  3.46 us
    ppermute x1, starting transfers between devices, padded_2(): before = lax.ppermute(last, axis, up)  2.4 us
  transfers between devices with their start and end apart: 2, of which 0 were waited for; matrix products, arithmetic and copies ran while one was open for 2% of the time, Pallas kernels for 87%

profile of v2, /device:TPU:0, one launch (start us, length us, event | category | flops | bytes accessed | tf_op | source)
XLA Modules:
  0.0 109.0 jit_solution(137883153595283153)
XLA Ops:
  0.6 0.0 copy-start
  0.6 0.0 copy-start.1
  0.7 1.2 %fusion.1 = f32[192]{0:T(256)S(1)} fusion(bf16[192,1024]{1,0:T(8,128)(2,1)} %param.11), kind=kLoop, calls=%fused_computation.7 | loop fusion | flops 589632 | bytes 393984 | tf_op jit(solution)/shard_map/reduce_sum | solution.py:30
  1.9 0.0 copy-done.1
  1.9 0.0 copy-start.2
  1.9 0.9 fusion.3
  2.8 2.4 %collective-permute-start = (bf16[8,1024]{1,0:T(8,128)(2,1)S(1)}, bf16[8,1024]{1,0:T(8,128)(2,1)S(1)}, u32[]{:S(2)}, u32[]{:S(2)}) collective-permute-start(bf16[8,1024]{1,0:T(8,128)(2,1)S(1)} %get-tuple-element.5), channel_id=1, source_target_pairs={{0,1},{1,2},{2,3},{3,4},{4,5},{5,6},{6,7},{7,8},{8,9},{9,10},{10,1... | collective-permute-start | bytes 49160 | tf_op jit(solution)/shard_map/ppermute | solution.py:22
  5.2 1.3 %collective-permute-start.1 = (bf16[8,1024]{1,0:T(8,128)(2,1)S(1)}, bf16[8,1024]{1,0:T(8,128)(2,1)S(1)}, u32[]{:S(2)}, u32[]{:S(2)}) collective-permute-start(bf16[8,1024]{1,0:T(8,128)(2,1)S(1)} %get-tuple-element.6), channel_id=1, source_target_pairs={{1,0},{2,1},{3,2},{4,3},{5,4},{6,5},{7,6},{8,7},{9,8},{10,9},{11,1... | collective-permute-start | bytes 49160 | tf_op jit(solution)/shard_map/ppermute | solution.py:23
  6.5 0.0 copy-start.4
  6.6 0.7 copy-done.4
  7.2 0.0 copy-start.7
  7.2 0.7 copy-done.7
  7.9 0.1 fusion
  8.1 0.0 copy-done.2
  8.1 0.2 fusion.4
  8.3 0.5 copy-done.5
  8.8 0.9 fusion.6.token_ref
  9.7 0.6 pad.4.table_ref
  10.3 95.2 %shard_map.122 = bf16[192,1024]{1,0:T(8,128)(2,1)} custom-call(bf16[192,1024]{1,0:T(8,128)(2,1)} %fusion.6.token_ref, bf16[16,256]{1,0:T(8,128)(2,1)} %pad.4.table_ref, bf16[1024,512]{1,0:T(8,128)(2,1)} %bitcast.20, bf16[1024,512]{1,0:T(8,128)(2,1)} %bitcast.21, bf16[512,1024]{1,0:T(8,128)(2,1)} %bitcast.22), custom_call_target="tpu_custom_call" | custom-call | tf_op jit(solution)/shard_map/pallas_call | solution.py:593
  105.6 0.0 collective-permute-done
  105.6 0.0 collective-permute-done.1
  105.6 0.1 maximum_convert_fusion
  105.7 0.2 fusion.32
  105.9 0.3 fusion.29
  106.2 0.0 copy-done
  106.2 0.3 convolution_bitcast_fusion
  106.5 0.0 copy-start.6
  106.5 0.1 copy.19
  106.6 0.6 copy-done.6
  107.2 0.8 multiply_convert_fusion
  108.0 0.2 copy-done.3
  108.3 0.7 copy.21
  (11 shorter events, 0.1 us)
Async XLA Ops:
  0.6 105.6 %copy-start = (bf16[4,256,256]{2,1,0:T(8,128)(2,1)S(1)}, bf16[4,256,256]{2,1,0:T(8,128)(2,1)}, u32[]{:S(2)}) copy-start(bf16[4,256,256]{2,1,0:T(8,128)(2,1)} %param.13) | copy-start | bytes 1572868
  0.6 1.3 %copy-start.1 = (bf16[192,1024]{1,0:T(8,128)(2,1)S(1)}, bf16[192,1024]{1,0:T(8,128)(2,1)}, u32[]{:S(2)}) copy-start(bf16[192,1024]{1,0:T(8,128)(2,1)} %param.11) | copy-start | bytes 1179652
  1.9 6.2 %copy-start.2 = (bf16[192,1024]{1,0:T(8,128)(2,1)S(1)}, bf16[192,1024]{1,0:T(8,128)(2,1)}, u32[]{:S(2)}) copy-start(bf16[192,1024]{1,0:T(8,128)(2,1)} %param.15) | copy-start | bytes 1179652
  2.8 102.8 %collective-permute-start = (bf16[8,1024]{1,0:T(8,128)(2,1)S(1)}, bf16[8,1024]{1,0:T(8,128)(2,1)S(1)}, u32[]{:S(2)}, u32[]{:S(2)}) collective-permute-start(bf16[8,1024]{1,0:T(8,128)(2,1)S(1)} %get-tuple-element.5), channel_id=1, source_target_pairs={{0,1},{1,2},{2,3},{3,4},{4,5},{5,6},{6,7},{7,8},{8,9},{9,10},{10,1... | collective-permute-start | bytes 49160 | tf_op jit(solution)/shard_map/ppermute | solution.py:22
  5.2 100.4 %collective-permute-start.1 = (bf16[8,1024]{1,0:T(8,128)(2,1)S(1)}, bf16[8,1024]{1,0:T(8,128)(2,1)S(1)}, u32[]{:S(2)}, u32[]{:S(2)}) collective-permute-start(bf16[8,1024]{1,0:T(8,128)(2,1)S(1)} %get-tuple-element.6), channel_id=1, source_target_pairs={{1,0},{2,1},{3,2},{4,3},{5,4},{6,5},{7,6},{8,7},{9,8},{10,9},{11,1... | collective-permute-start | bytes 49160 | tf_op jit(solution)/shard_map/ppermute | solution.py:23
  6.5 0.7 copy-start.4
  7.2 0.7 copy-start.7
  8.1 0.7 copy-start.5
  106.5 0.7 copy-start.6
  107.2 1.1 copy-start.3

commit v3 on v2

--- a/solution.py
+++ b/solution.py
@@ -10,6 +10,7 @@
 
 epsilon = 1e-06
 vmem_share = 2**24
+edge = 8
 
 
 def padded_2(value, sides, width):
@@ -116,44 +117,34 @@
     return expert_out
 
 
-def slots(routes, route_weight, experts):
-    chosen = routes[:, :, None] == jnp.arange(experts, dtype=jnp.int32)[None, None, :]
-    named = jnp.any(chosen, axis=1)
-    weight = jnp.sum(jnp.where(chosen, route_weight[:, :, None], 0.0), axis=1)
-    rows = routes.shape[0]
-    earlier = jnp.arange(rows)[None, :] < jnp.arange(rows)[:, None]
-    place = jnp.dot(
-        earlier.astype(jnp.bfloat16), named.astype(jnp.bfloat16), preferred_element_type=jnp.float32
-    )
-    place = jnp.where(named, place, -1.0)
-    high = lax.reduce_precision(weight, 8, 7)
-    return jnp.concatenate([place, high, weight - high], axis=1).T.astype(jnp.bfloat16)
-
-
 ORDERS = (
     (
-        ("D", 0, 1), ("D", 0, 0), ("X", 0, 0), ("Y", 0, 0), ("M", 0, 0), ("D", 1, 0), ("G", 0, 0),
-        ("D", 1, 1), ("M", 1, 0), ("D", 2, 1), ("D", 2, 0), ("C", 0, 0), ("M", 2, 0), ("C", 2, 0),
-        ("I", 0, 0), ("C", 0, 2), ("C", 0, 1), ("D", 3, 1), ("D", 3, 0), ("M", 3, 0), ("I", 2, 0),
-        ("G", 1, 0), ("P", 0, 1), ("C", 2, 2), ("C", 1, 3), ("C", 2, 1), ("I", 3, 0), ("F", 1, 0),
-        ("I", 1, 0), ("G", 2, 0), ("C", 3, 2), ("F", 1, 1), ("C", 2, 3), ("C", 3, 1), ("F", 2, 0),
-        ("P", 3, 2), ("C", 1, 2), ("P", 2, 2), ("P", 3, 1), ("P", 2, 1), ("F", 2, 1), ("G", 3, 0),
-        ("C", 3, 3), ("C", 1, 0), ("F", 3, 0), ("F", 3, 1), ("C", 3, 0), ("C", 0, 3), ("C", 1, 1),
-        ("E", 3, 0), ("P", 1, 2), ("P", 1, 1), ("P", 0, 2), ("S", 3, 0), ("S", 3, 1), ("E", 2, 0),
-        ("S", 2, 0), ("S", 2, 1), ("F", 0, 0), ("E", 1, 0), ("S", 1, 0), ("F", 0, 1), ("V", 0, 0),
-        ("V", 0, 1), ("E", 0, 0), ("S", 1, 1), ("S", 0, 0), ("S", 0, 1), ("Z", 0, 0),
+        ("D", 0, 0), ("D", 0, 1), ("X", 0, 0), ("M", 0, 0), ("D", 1, 1), ("Y", 0, 0), ("I", 0, 0),
+        ("D", 1, 0), ("M", 1, 0), ("D", 2, 0), ("D", 2, 1), ("G", 0, 0), ("M", 2, 0), ("I", 1, 0),
+        ("C", 1, 1), ("C", 1, 2), ("C", 2, 0), ("G", 1, 0), ("P", 1, 1), ("P", 1, 2), ("C", 0, 3),
+        ("C", 0, 2), ("D", 3, 1), ("C", 1, 3), ("I", 2, 0), ("C", 0, 1), ("D", 3, 0), ("M", 3, 0),
+        ("C", 1, 0), ("F", 1, 0), ("P", 0, 1), ("C", 2, 1), ("C", 0, 0), ("F", 1, 1), ("P", 0, 2),
+        ("E", 1, 0), ("G", 2, 0), ("S", 1, 1), ("C", 2, 2), ("C", 2, 3), ("P", 2, 1), ("I", 3, 0),
+        ("F", 2, 0), ("C", 3, 2), ("P", 2, 2), ("G", 3, 0), ("C", 3, 1), ("P", 3, 2), ("F", 2, 1),
+        ("C", 3, 3), ("E", 0, 0), ("F", 3, 0), ("F", 3, 1), ("C", 3, 0), ("P", 3, 1), ("H", 0, 0),
+        ("E", 2, 0), ("S", 2, 3), ("S", 2, 2), ("E", 3, 0), ("S", 3, 1), ("S", 3, 2), ("S", 3, 0),
+        ("S", 3, 3), ("Q", 0, 0), ("F", 0, 0), ("S", 2, 0), ("Q", 0, 1), ("Q", 0, 3), ("Q", 0, 2),
+        ("S", 2, 1), ("S", 1, 3), ("S", 1, 0), ("S", 1, 2), ("F", 0, 1), ("V", 0, 0), ("S", 0, 1),
+        ("V", 0, 1), ("S", 0, 3), ("S", 0, 2), ("S", 0, 0), ("Z", 0, 0),
     ),
     (
-        ("D", 1, 0), ("D", 1, 1), ("X", 1, 0), ("M", 1, 0), ("Y", 1, 0), ("D", 2, 0), ("D", 0, 0),
-        ("D", 2, 1), ("I", 1, 0), ("D", 0, 1), ("M", 0, 0), ("D", 3, 0), ("C", 1, 1), ("D", 3, 1),
-        ("M", 3, 0), ("I", 0, 0), ("G", 1, 0), ("C", 0, 1), ("P", 0, 1), ("C", 1, 3), ("G", 0, 0),
-        ("I", 3, 0), ("G", 2, 0), ("C", 0, 3), ("C", 3, 2), ("M", 2, 0), ("C", 3, 1), ("P", 3, 2),
-        ("C", 0, 2), ("G", 3, 0), ("P", 3, 1), ("C", 1, 2), ("C", 2, 0), ("C", 1, 0), ("C", 3, 3),
-        ("I", 2, 0), ("C", 2, 3), ("P", 0, 2), ("P", 1, 1), ("C", 2, 2), ("C", 2, 1), ("C", 0, 0),
-        ("P", 1, 2), ("F", 2, 0), ("F", 2, 1), ("C", 3, 0), ("F", 3, 0), ("F", 1, 0), ("P", 2, 2),
-        ("F", 3, 1), ("P", 2, 1), ("F", 0, 0), ("E", 3, 0), ("S", 3, 0), ("E", 1, 0), ("E", 0, 0),
-        ("F", 1, 1), ("V", 1, 0), ("F", 0, 1), ("S", 3, 1), ("E", 2, 0), ("S", 0, 0), ("S", 2, 0),
-        ("S", 0, 1), ("S", 2, 1), ("V", 1, 1), ("S", 1, 0), ("S", 1, 1), ("Z", 1, 0),
+        ("D", 1, 1), ("D", 1, 0), ("X", 1, 0), ("Y", 1, 0), ("D", 2, 1), ("D", 0, 0), ("D", 0, 1),
+        ("D", 2, 0), ("G", 1, 0), ("M", 0, 0), ("M", 2, 0), ("D", 3, 1), ("M", 1, 0), ("C", 1, 3),
+        ("D", 3, 0), ("I", 2, 0), ("G", 0, 0), ("C", 2, 1), ("C", 2, 2), ("G", 2, 0), ("C", 1, 0),
+        ("M", 3, 0), ("I", 1, 0), ("P", 2, 1), ("I", 0, 0), ("C", 1, 2), ("P", 2, 2), ("G", 3, 0),
+        ("C", 2, 3), ("C", 0, 2), ("I", 3, 0), ("C", 0, 1), ("C", 3, 2), ("C", 2, 0), ("C", 3, 1),
+        ("P", 0, 2), ("F", 2, 0), ("C", 3, 3), ("P", 3, 1), ("E", 2, 0), ("P", 0, 1), ("F", 2, 1),
+        ("P", 3, 2), ("C", 1, 1), ("F", 1, 0), ("F", 3, 0), ("C", 0, 0), ("C", 0, 3), ("F", 3, 1),
+        ("P", 1, 1), ("C", 3, 0), ("S", 2, 3), ("F", 1, 1), ("E", 3, 0), ("S", 2, 2), ("F", 0, 0),
+        ("P", 1, 2), ("H", 1, 0), ("S", 3, 1), ("E", 0, 0), ("F", 0, 1), ("S", 3, 2), ("Q", 1, 0),
+        ("V", 1, 0), ("S", 0, 1), ("S", 3, 0), ("S", 0, 2), ("S", 3, 3), ("S", 0, 0), ("Q", 1, 3),
+        ("S", 2, 0), ("Q", 1, 2), ("Q", 1, 1), ("V", 1, 1), ("S", 0, 3), ("S", 2, 1), ("E", 1, 0),
+        ("S", 1, 3), ("S", 1, 1), ("S", 1, 0), ("S", 1, 2), ("Z", 1, 0),
     ),
 )
 
@@ -177,8 +168,9 @@
 
 def stream_kernel(
     depth, capacity, experts,
-    token_ref, table_ref, gate_ref, up_ref, down_ref, out_ref,
-    tok, tables, blk, part, from_core, out_right, out_left, out_far, relay_right, relay_left,
+    input_ref, gain_ref, routes_ref, weight_ref, mixer_gain_ref, mixer_scale_ref,
+    gate_hbm, up_hbm, down_hbm, mixer_hbm, group_hbm, mixed_ref, out_ref,
+    gate_ref, up_ref, down_ref, mixer_ref, group_ref, mix, tok, tables, blk, part, from_core, out_right, out_left, out_far, relay_right, relay_left,
     from_right, from_left, local, dense, dense_above, dense_below,
     far_above, far_below, home_left, home_right, far_back,
     send_sem, recv_sem, local_sem,
@@ -187,10 +179,10 @@
     level, core = line // 2, line % 2
     other = 1 - core
     rows = out_ref.shape[0]
-    half = rows // 2
+    half, quarter = rows // 2, rows // 4
     low = -(-capacity // 32) * 16
     high = capacity - low
-    piece = math.gcd(half, capacity)
+    piece = math.gcd(quarter, capacity)
     step_rows = math.gcd(low, high)
     right_column, left_column, far_column = (2 * column + 1) % 5, (3 * column + 2) % 5, 3 - column
     right, left = (right_column, line), (left_column, line)
@@ -260,31 +252,63 @@
     def back_right(at):
         return link(part.at[at, 2, core], from_left.at[at], 23, at, right)
 
+    def fourth(h):
+        return pl.ds(pl.multiple_of(h * quarter, quarter), quarter)
+
     def sum_down(at, h):
-        return link(dense.at[at, part_of(h)], dense_above.at[at, part_of(h)], 24 + h, at, below)
+        return link(dense.at[at, fourth(h)], dense_above.at[at, fourth(h)], 24 + h, at, below)
 
     def sum_up(at, h):
-        return link(dense.at[at, part_of(h)], dense_below.at[at, part_of(h)], 26 + h, at, above)
+        return link(dense.at[at, fourth(h)], dense_below.at[at, fourth(h)], 28 + h, at, above)
 
     cuts = (pl.ds(0, low), pl.ds(low, high))
 
     def far_sum_down(at, h):
-        return link(part.at[at, 3, core, cuts[h]], far_above.at[at, cuts[h]], 28 + h, at, below)
+        return link(part.at[at, 3, core, cuts[h]], far_above.at[at, cuts[h]], 32 + h, at, below)
 
     def far_sum_up(at, h):
-        return link(part.at[at, 3, core, cuts[h]], far_below.at[at, cuts[h]], 30 + h, at, above)
+        return link(part.at[at, 3, core, cuts[h]], far_below.at[at, cuts[h]], 34 + h, at, above)
 
     def home_low():
-        return link(part.at[level, 3, core, cuts[0]], home_left, 32, 0, left)
+        return link(part.at[level, 3, core, cuts[0]], home_left, 36, 0, left)
 
     def home_high():
-        return link(part.at[level, 3, core, cuts[1]], home_right, 33, 0, right)
+        return link(part.at[level, 3, core, cuts[1]], home_right, 37, 0, right)
 
     def last_low():
-        return link(home_left, far_back.at[cuts[0]], 34, 0, left)
+        return link(home_left, far_back.at[cuts[0]], 38, 0, left)
 
     def last_high():
-        return link(home_right, far_back.at[cuts[1]], 35, 0, right)
+        return link(home_right, far_back.at[cuts[1]], 39, 0, right)
+
+    place = column * 2 * depth + line
+    last_place = lax.axis_size("ep") * 2 * depth - 1
+    first_line, last_line = line == 0, line == 2 * depth - 1
+    following = (column + jnp.where(last_line, 1, 0), jnp.where(last_line, 0, line + 1))
+    preceding = (column - jnp.where(first_line, 1, 0), jnp.where(first_line, 2 * depth - 1, line - 1))
+    has_following, has_preceding = place < last_place, place > 0
+
+    def to_following():
+        return link(mix.at[pl.ds(rows, edge)], mix.at[pl.ds(0, edge)], 40, 0, following)
+
+    def to_preceding():
+        return link(
+            mix.at[pl.ds(edge, edge)], mix.at[pl.ds(edge + rows, edge)], 41, 0, preceding
+        )
+
+    loads = [
+        pltpu.make_async_copy(src, dst, local_sem.at[n])
+        for n, (src, dst) in enumerate((
+            (gate_hbm, gate_ref), (up_hbm, up_ref), (down_hbm, down_ref),
+            (mixer_hbm, mixer_ref), (group_hbm, group_ref),
+        ))
+    ]
+    def by_piece(start, count, width, body):
+        def one(i, carry):
+            body(pl.ds(pl.multiple_of(start + i * width, width), width))
+            return carry
+
+        lax.fori_loop(0, count // width, one, 0)
 
     barrier = pltpu.get_barrier_semaphore()
 
@@ -298,12 +322,41 @@
     greet(beside)
     pl.when(has_above)(lambda: greet(above))
     pl.when(has_below)(lambda: greet(below))
-    own_copy = pltpu.make_async_copy(token_ref, tok.at[level], local_sem)
-    own_copy.start()
-    own_copy.wait()
-    own_table = pltpu.make_async_copy(table_ref, tables.at[level], local_sem)
-    own_table.start()
-    own_table.wait()
+    for load in loads:
+        load.start()
+
+    def normed(values, gains):
+        values = values.astype(f32)
+        mean = jnp.sum(values * values, axis=1, keepdims=True) / values.shape[1]
+        return (values * lax.rsqrt(mean + epsilon) * gains).astype(bf16)
+
+    def own_rows(span):
+        tok[level, span] = normed(input_ref[span], gain_ref[...])
+
+    by_piece(0, rows, piece, own_rows)
+    sort = lax.broadcasted_iota(jnp.int32, (tables.shape[1], rows), 0)
+    first = sort % experts == routes_ref[0:1, :]
+    second = sort % experts == routes_ref[1:2, :]
+    weights = jnp.where(first, weight_ref[0:1, :], 0.0) + jnp.where(second, weight_ref[1:2, :], 0.0)
+    named = first | second
+    earlier = lax.broadcasted_iota(jnp.int32, (rows, rows), 0) < lax.broadcasted_iota(
+        jnp.int32, (rows, rows), 1
+    )
+    turns = jnp.dot(
+        jnp.where(named, 1.0, 0.0).astype(bf16), jnp.where(earlier, 1.0, 0.0).astype(bf16),
+        preferred_element_type=f32,
+    )
+    turns = jnp.where(named, turns, -1.0).astype(bf16)
+    coarse = weights.astype(bf16)
+    fine = (weights - coarse.astype(f32)).astype(bf16)
+    group = sort // experts
+    listed = jnp.where(
+        group == 0, turns.astype(f32), jnp.where(group == 1, coarse.astype(f32), fine.astype(f32))
+    )
+    tables[level, :, pl.ds(0, rows)] = listed.astype(bf16)
+    tables[level, :, pl.ds(rows, tables.shape[2] - rows)] = jnp.zeros(
+        (tables.shape[1], tables.shape[2] - rows), bf16
+    )
     pl.semaphore_wait(barrier, 3 + jnp.where(has_above, 1, 0) + jnp.where(has_below, 1, 0))
 
     def table(at):
@@ -350,13 +403,6 @@
         for lane in range(2):
             part[at, q, lane] = partial[lane * capacity : (lane + 1) * capacity]
 
-    def by_piece(start, count, width, body):
-        def one(i, carry):
-            body(pl.ds(pl.multiple_of(start + i * width, width), width))
-            return carry
-
-        lax.fori_loop(0, count // width, one, 0)
-
     def paired(at, q):
         give(at, q).wait_recv()
 
@@ -413,7 +459,7 @@
                     total = total + dense_below[at, span].astype(f32)
                 dense[at, span] = total.astype(bf16)
 
-            by_piece(h * half, half, piece, body)
+            by_piece(h * quarter, quarter, piece, body)
 
         with_incoming(above_too, below_too, action)
         pl.when(at < level)(lambda: sum_down(at, h).start())
@@ -446,6 +492,8 @@
         out_far[...] = picked(at, (far_column,))
         far_right().start()
         far_left().start()
+        for load in loads[:3]:
+            load.wait()
 
     def relay(at, _):
         far_right().wait_recv()
@@ -507,10 +555,61 @@
         total = placed(level, (far_column,), far_back[...])
         out_ref[...] = (dense[level].astype(f32) + total).astype(bf16)
 
+    def mixer_rows(at, _):
+        for load in loads[3:]:
+            load.wait()
+
+        def body(i, carry):
+            start = pl.multiple_of(i * piece, piece)
+            values = normed(mixer_ref[pl.ds(start, piece)], mixer_gain_ref[...])
+            mix[pl.ds(pl.multiple_of(start + edge, edge), piece)] = values.astype(f32)
+            return carry
+
+        lax.fori_loop(0, rows // piece, body, 0)
+        zeros = jnp.zeros((edge, mix.shape[1]), f32)
+
+        @pl.when(jnp.logical_not(has_preceding))
+        def _():
+            mix[pl.ds(0, edge)] = zeros
+
+        @pl.when(jnp.logical_not(has_following))
+        def _():
+            mix[pl.ds(edge + rows, edge)] = zeros
+
+        pl.when(has_following)(lambda: to_following().start())
+        pl.when(has_preceding)(lambda: to_preceding().start())
+
+    def mixer_group(number):
+        width = group_ref.shape[1]
+        span = pl.ds(number * width, width)
+        window = 2 ** (number + 1)
+        values = mix[:, span]
+        length = values.shape[0]
+        total = values
+        for level_of_sum in range(number + 1):
+            total = total + pltpu.roll(total, length - 2**level_of_sum, 0)
+        total = pltpu.roll(total, window // 2, 0)[edge : edge + rows]
+        position = place * rows + lax.broadcasted_iota(jnp.int32, (rows, width), 0)
+        ahead = jnp.minimum(position + window // 2, (last_place + 1) * rows)
+        cover = (ahead - jnp.maximum(position - window // 2, 0)).astype(f32)
+        pooled = (total / cover - values[edge : edge + rows]).astype(bf16)
+        product = jnp.dot(pooled, group_ref[number], preferred_element_type=f32)
+        mixed_ref[:, span] = (product * mixer_scale_ref[:, span]).astype(bf16)
+
+    def mixer_step(at, q):
+        @pl.when(q == 0)
+        def _():
+            pl.when(has_preceding)(lambda: to_following().wait_recv())
+            pl.when(has_following)(lambda: to_preceding().wait_recv())
+
+        for number in range(4):
+            pl.when(q == number)(functools.partial(mixer_group, number))
+
     actions = dict(
         D=arrive, M=sides_out, I=sides_in, G=far_in,
         C=multiply, P=back, F=far_step, S=dense_step,
         E=expand, X=far_out, Y=relay, V=home_relay, Z=finish,
+        H=mixer_rows, Q=mixer_step,
     )
     kinds = list(actions)
     words, per_word, base = coded_orders(depth, kinds)
@@ -556,10 +655,11 @@
         for h in range(2):
             settle(upward, up, h)
             settle(downward, down, h)
+            settle(at < level, far_sum_down, h)
+            settle(at > level, far_sum_up, h)
+        for h in range(4):
             settle(at < level, sum_down, h)
             settle(at > level, sum_up, h)
-            settle(at < level, far_sum_down, h)
-            settle(at > level, far_sum_up, h)
         for copy in (to_right, to_left, back_left, back_right):
             copy(at).wait_send()
         for q in range(4):
@@ -572,31 +672,37 @@
         far_right, far_left, on_right, on_left, home_low, home_high, last_low, last_high
     ):
         copy().wait_send()
-
-
-def dense_plan(expert_input, expert_gain, routes, route_weight, w_gate, w_up, w_down):
+    pl.when(has_following)(lambda: to_following().wait_send())
+    pl.when(has_preceding)(lambda: to_preceding().wait_send())
+
+
+def dense_plan(
+    mixer_input, mixer_gain, group_weight, mixer_scale,
+    expert_input, expert_gain, routes, route_weight, w_gate, w_up, w_down,
+):
     row_count, width = expert_input.shape
     experts = lax.axis_size("ep")
     depth = lax.axis_size("tp") // 2
     capacity = 3 * routes.shape[1] * row_count // (2 * experts)
-    normed = normalize(expert_input, expert_gain)
-    listed = slots(routes, route_weight, experts)
     pad = -(-3 * experts // 16) * 16
     lanes = -(-row_count // 128) * 128
-    listed = jnp.pad(listed, ((0, pad - 3 * experts), (0, lanes - row_count)))
-    bf16 = jnp.bfloat16
+    bf16, f32 = jnp.bfloat16, jnp.float32
     low = -(-capacity // 32) * 16
     high = capacity - low
-    vmem = pl.BlockSpec(memory_space=pltpu.VMEM)
+    vmem, anywhere = pl.BlockSpec(memory_space=pltpu.VMEM), pl.BlockSpec(memory_space=pl.ANY)
     compact = pltpu.VMEM((depth, capacity, width), bf16)
     dense = pltpu.VMEM((depth, row_count, width), bf16)
+    result = jax.ShapeDtypeStruct((row_count, width), bf16)
+    stationary = (w_gate[0], w_up[0], w_down[0], mixer_input, group_weight)
     return pl.pallas_call(
         functools.partial(stream_kernel, depth, capacity, experts),
-        out_shape=jax.ShapeDtypeStruct((row_count, width), bf16),
-        in_specs=[vmem] * 5,
-        out_specs=vmem,
+        out_shape=(result, result),
+        in_specs=[vmem] * 6 + [anywhere] * 5,
+        out_specs=(vmem, vmem),
         scratch_shapes=[
-            pltpu.VMEM((depth, row_count, width), bf16),
+            *(pltpu.VMEM(array.shape, bf16) for array in stationary),
+            pltpu.VMEM((row_count + 2 * edge, width), f32),
+            dense,
             pltpu.VMEM((depth, pad, lanes), bf16),
             pltpu.VMEM((depth, 4, 2, capacity, width), bf16),
             pltpu.VMEM((depth, 4, 2, capacity, width), bf16),
@@ -608,7 +714,7 @@
             pltpu.VMEM((high, width), bf16),
             compact,
             compact,
-            pltpu.VMEM((depth, row_count, width), jnp.float32),
+            pltpu.VMEM((depth, row_count, width), f32),
             dense,
             dense,
             dense,
@@ -617,14 +723,17 @@
             pltpu.VMEM((low, width), bf16),
             pltpu.VMEM((high, width), bf16),
             pltpu.VMEM((capacity, width), bf16),
-            pltpu.SemaphoreType.DMA((36, depth)),
-            pltpu.SemaphoreType.DMA((36, depth)),
-            pltpu.SemaphoreType.DMA,
+            pltpu.SemaphoreType.DMA((42, depth)),
+            pltpu.SemaphoreType.DMA((42, depth)),
+            pltpu.SemaphoreType.DMA((len(stationary),)),
         ],
         compiler_params=pltpu.CompilerParams(
             collective_id=0, has_side_effects=True, vmem_limit_bytes=60 * 2**20
         ),
-    )(normed, listed, w_gate[0], w_up[0], w_down[0])
+    )(
+        expert_input, expert_gain.reshape(1, -1), routes.T, route_weight.T,
+        mixer_gain.reshape(1, -1), mixer_scale.reshape(1, -1), *stationary,
+    )
 
 
 def on_device(
@@ -634,8 +743,14 @@
     devices = lax.axis_size(("ep", "tp"))
     gathered_bytes = 2 * devices * expert_input.size
     square = lax.axis_size("ep") == 4 and lax.axis_size("tp") == 4 * len(ORDERS)
-    plan = dense_plan if square and gathered_bytes <= vmem_share else routed_plan
-    expert_out = plan(expert_input, expert_gain, routes, route_weight, w_gate, w_up, w_down)
+    if square and gathered_bytes <= vmem_share:
+        return dense_plan(
+            mixer_input, mixer_gain, group_weight, mixer_scale,
+            expert_input, expert_gain, routes, route_weight, w_gate, w_up, w_down,
+        )
+    expert_out = routed_plan(
+        expert_input, expert_gain, routes, route_weight, w_gate, w_up, w_down
+    )
     return (mixer(mixer_input, mixer_gain, group_weight, mixer_scale), expert_out)
 
 

time: 111 us -> 97.2 us (0.88); the launches traced: 109 us -> 97 us
  other arithmetic: 4.7 us -> 0 us
  starting transfers between devices: 3.69 us -> 0 us
  local copies, waits for them, and re-layouts: 4.15 us -> 2.57 us
  Pallas kernels: 95.2 us -> 93.8 us
    ppermute x2 -> x0, starting transfers between devices: 3.69 us -> none  [the longest x1 2.4 us: padded_2(): before = lax.ppermute(last, axis, up)]
    convert_element_type x7 -> x0, other arithmetic: 2.73 us -> none  [the longest x2 1.8 us: normalize(): return (scaled * gain).astype(jnp.bfloat16)]
    reduce_sum x3 -> x0, other arithmetic: 1.42 us -> none  [the longest x2 1.41 us: normalize(): jnp.mean(values * values, axis=-1, keepdims=True) + epsilon]
    pallas_call x1, Pallas kernels: 95.2 us -> 93.8 us  [dense_plan(): pl.pallas_call(functools.partial(stream_kernel, depth, capacity, experts)...]
    unnamed x17 -> x4, local copies, waits for them, and re-layouts: 3.46 us -> 2.57 us
  transfers between devices with their start and end apart: 2 -> 0, of which waited for: 0 -> 0; matrix products, arithmetic and copies ran while one was open for 2% -> 0% of each run, Pallas kernels for 87% -> 0%
where the time goes in v3:
time: 97.2 us; the launch traced here: 97 us
  Pallas kernels  93.8 us (97%)
  local copies, waits for them, and re-layouts  2.57 us (3%)
    pallas_call x1, Pallas kernels, dense_plan(): pl.pallas_call(functools.partial(stream_kernel, depth, capacity, experts)...  93.8 us
    unnamed x4, local copies, waits for them, and re-layouts  2.57 us

profile of v3, /device:TPU:0, one launch (start us, length us, event | category | flops | bytes accessed | tf_op | source)
XLA Modules:
  0.0 97.0 jit_solution(9397871423577872436)
XLA Ops:
  0.6 93.8 %shard_map.122 = (bf16[192,1024]{1,0:T(8,128)(2,1)}, bf16[192,1024]{1,0:T(8,128)(2,1)}) custom-call(bf16[192,1024]{1,0:T(8,128)(2,1)} %input_ref.1, f32[1,1024]{1,0:T(1,128)} %bitcast.11, s32[2,192]{1,0:T(2,128)} %bitcast.14, f32[2,192]{1,0:T(2,128)} %bitcast.15, f32[1,1024]{1,0:T(1,128)} %bitcast.12, f32[1,1024]{1,0:T(1,128)} %bitcast.13, ...), custom_call_target="tpu_custom_call" | custom-call | tf_op jit(solution)/shard_map/pallas_call | solution.py:697
  94.5 0.0 copy-start
  94.5 1.8 %copy.15 = bf16[192,1024]{1,0:T(8,128)(2,1)} copy(bf16[192,1024]{1,0:T(8,128)(2,1)} %get-tuple-element.4) | data formatting | bytes 786432
  96.3 0.0 copy-done
  96.3 0.7 copy.16
Async XLA Ops:
  94.5 1.8 %copy-start = (bf16[192,1024]{1,0:T(8,128)(2,1)S(1)}, bf16[192,1024]{1,0:T(8,128)(2,1)}, u32[]{:S(2)}) copy-start(bf16[192,1024]{1,0:T(8,128)(2,1)} %get-tuple-element.5) | copy-start | bytes 1179652

commit v4 on v3

--- a/solution.py
+++ b/solution.py
@@ -119,32 +119,35 @@
 
 ORDERS = (
     (
-        ("D", 0, 0), ("D", 0, 1), ("X", 0, 0), ("M", 0, 0), ("D", 1, 1), ("Y", 0, 0), ("I", 0, 0),
-        ("D", 1, 0), ("M", 1, 0), ("D", 2, 0), ("D", 2, 1), ("G", 0, 0), ("M", 2, 0), ("I", 1, 0),
-        ("C", 1, 1), ("C", 1, 2), ("C", 2, 0), ("G", 1, 0), ("P", 1, 1), ("P", 1, 2), ("C", 0, 3),
-        ("C", 0, 2), ("D", 3, 1), ("C", 1, 3), ("I", 2, 0), ("C", 0, 1), ("D", 3, 0), ("M", 3, 0),
-        ("C", 1, 0), ("F", 1, 0), ("P", 0, 1), ("C", 2, 1), ("C", 0, 0), ("F", 1, 1), ("P", 0, 2),
-        ("E", 1, 0), ("G", 2, 0), ("S", 1, 1), ("C", 2, 2), ("C", 2, 3), ("P", 2, 1), ("I", 3, 0),
-        ("F", 2, 0), ("C", 3, 2), ("P", 2, 2), ("G", 3, 0), ("C", 3, 1), ("P", 3, 2), ("F", 2, 1),
-        ("C", 3, 3), ("E", 0, 0), ("F", 3, 0), ("F", 3, 1), ("C", 3, 0), ("P", 3, 1), ("H", 0, 0),
-        ("E", 2, 0), ("S", 2, 3), ("S", 2, 2), ("E", 3, 0), ("S", 3, 1), ("S", 3, 2), ("S", 3, 0),
-        ("S", 3, 3), ("Q", 0, 0), ("F", 0, 0), ("S", 2, 0), ("Q", 0, 1), ("Q", 0, 3), ("Q", 0, 2),
-        ("S", 2, 1), ("S", 1, 3), ("S", 1, 0), ("S", 1, 2), ("F", 0, 1), ("V", 0, 0), ("S", 0, 1),
-        ("V", 0, 1), ("S", 0, 3), ("S", 0, 2), ("S", 0, 0), ("Z", 0, 0),
+        ("D", 0, 1), ("D", 0, 0), ("X", 0, 0), ("Y", 0, 0), ("M", 0, 0), ("C", 0, 0), ("D", 1, 1),
+        ("D", 1, 0), ("M", 1, 0), ("G", 0, 0), ("C", 0, 3), ("I", 0, 0), ("D", 2, 0), ("D", 2, 1),
+        ("M", 2, 0), ("C", 0, 2), ("I", 1, 0), ("C", 2, 0), ("C", 1, 0), ("K", 0, 0), ("D", 3, 0),
+        ("D", 3, 1), ("M", 3, 0), ("C", 0, 1), ("I", 2, 0), ("C", 1, 2), ("C", 2, 1), ("G", 1, 0),
+        ("C", 2, 2), ("P", 2, 1), ("C", 1, 3), ("P", 2, 2), ("I", 3, 0), ("K", 1, 0), ("C", 1, 1),
+        ("F", 1, 0), ("G", 3, 0), ("F", 1, 1), ("C", 3, 2), ("C", 3, 3), ("C", 3, 1), ("F", 3, 0),
+        ("F", 3, 1), ("K", 3, 0), ("E", 2, 0), ("S", 2, 1), ("G", 2, 0), ("P", 3, 1), ("S", 2, 2),
+        ("S", 2, 0), ("P", 3, 2), ("C", 2, 3), ("F", 2, 0), ("K", 2, 0), ("V", 3, 0), ("P", 1, 1),
+        ("C", 3, 0), ("V", 3, 1), ("P", 1, 2), ("F", 2, 1), ("L", 2, 0), ("F", 0, 0), ("S", 2, 3),
+        ("H", 0, 0), ("P", 0, 2), ("E", 3, 0), ("S", 3, 0), ("S", 3, 2), ("Q", 0, 0), ("F", 0, 1),
+        ("S", 3, 1), ("L", 3, 0), ("S", 3, 3), ("Q", 0, 1), ("P", 0, 1), ("E", 1, 0), ("S", 1, 1),
+        ("S", 1, 2), ("L", 1, 0), ("S", 1, 0), ("Q", 0, 3), ("S", 1, 3), ("Q", 0, 2), ("V", 0, 0),
+        ("V", 0, 1), ("E", 0, 0), ("S", 0, 1), ("L", 0, 0), ("S", 0, 2), ("S", 0, 0), ("S", 0, 3),
+        ("Z", 0, 0),
     ),
     (
-        ("D", 1, 1), ("D", 1, 0), ("X", 1, 0), ("Y", 1, 0), ("D", 2, 1), ("D", 0, 0), ("D", 0, 1),
-        ("D", 2, 0), ("G", 1, 0), ("M", 0, 0), ("M", 2, 0), ("D", 3, 1), ("M", 1, 0), ("C", 1, 3),
-        ("D", 3, 0), ("I", 2, 0), ("G", 0, 0), ("C", 2, 1), ("C", 2, 2), ("G", 2, 0), ("C", 1, 0),
-        ("M", 3, 0), ("I", 1, 0), ("P", 2, 1), ("I", 0, 0), ("C", 1, 2), ("P", 2, 2), ("G", 3, 0),
-        ("C", 2, 3), ("C", 0, 2), ("I", 3, 0), ("C", 0, 1), ("C", 3, 2), ("C", 2, 0), ("C", 3, 1),
-        ("P", 0, 2), ("F", 2, 0), ("C", 3, 3), ("P", 3, 1), ("E", 2, 0), ("P", 0, 1), ("F", 2, 1),
-        ("P", 3, 2), ("C", 1, 1), ("F", 1, 0), ("F", 3, 0), ("C", 0, 0), ("C", 0, 3), ("F", 3, 1),
-        ("P", 1, 1), ("C", 3, 0), ("S", 2, 3), ("F", 1, 1), ("E", 3, 0), ("S", 2, 2), ("F", 0, 0),
-        ("P", 1, 2), ("H", 1, 0), ("S", 3, 1), ("E", 0, 0), ("F", 0, 1), ("S", 3, 2), ("Q", 1, 0),
-        ("V", 1, 0), ("S", 0, 1), ("S", 3, 0), ("S", 0, 2), ("S", 3, 3), ("S", 0, 0), ("Q", 1, 3),
-        ("S", 2, 0), ("Q", 1, 2), ("Q", 1, 1), ("V", 1, 1), ("S", 0, 3), ("S", 2, 1), ("E", 1, 0),
-        ("S", 1, 3), ("S", 1, 1), ("S", 1, 0), ("S", 1, 2), ("Z", 1, 0),
+        ("D", 1, 0), ("D", 1, 1), ("X", 1, 0), ("M", 1, 0), ("D", 0, 1), ("D", 2, 0), ("Y", 1, 0),
+        ("D", 2, 1), ("M", 2, 0), ("D", 0, 0), ("C", 1, 0), ("I", 1, 0), ("D", 3, 1), ("C", 1, 1),
+        ("M", 0, 0), ("C", 1, 2), ("D", 3, 0), ("C", 2, 0), ("M", 3, 0), ("G", 0, 0), ("C", 0, 0),
+        ("I", 2, 0), ("G", 1, 0), ("P", 1, 2), ("P", 1, 1), ("C", 2, 1), ("C", 0, 3), ("I", 0, 0),
+        ("C", 2, 2), ("G", 3, 0), ("C", 0, 1), ("C", 0, 2), ("C", 3, 3), ("K", 0, 0), ("P", 2, 1),
+        ("C", 3, 0), ("G", 2, 0), ("F", 3, 0), ("I", 3, 0), ("C", 1, 3), ("F", 3, 1), ("C", 2, 3),
+        ("P", 2, 2), ("C", 3, 1), ("C", 3, 2), ("P", 0, 1), ("K", 1, 0), ("H", 1, 0), ("E", 1, 0),
+        ("K", 2, 0), ("F", 0, 0), ("K", 3, 0), ("P", 3, 1), ("P", 3, 2), ("P", 0, 2), ("E", 2, 0),
+        ("L", 2, 0), ("F", 0, 1), ("S", 2, 1), ("L", 1, 0), ("S", 2, 0), ("S", 2, 2), ("F", 2, 0),
+        ("Q", 1, 0), ("F", 2, 1), ("E", 0, 0), ("E", 3, 0), ("S", 3, 0), ("F", 1, 0), ("Q", 1, 1),
+        ("S", 3, 2), ("F", 1, 1), ("L", 0, 0), ("L", 3, 0), ("Q", 1, 3), ("S", 3, 1), ("S", 0, 0),
+        ("Q", 1, 2), ("S", 3, 3), ("S", 0, 2), ("S", 2, 3), ("S", 0, 1), ("V", 1, 1), ("V", 1, 0),
+        ("S", 0, 3), ("S", 1, 0), ("S", 1, 2), ("S", 1, 3), ("S", 1, 1), ("Z", 1, 0),
     ),
 )
 
@@ -155,10 +158,12 @@
     while base ** (per_word + 1) < 2**31:
         per_word += 1
     idle = base - 1
+    longest = max(map(len, ORDERS))
+    longest += -longest % per_word
     words = []
     for order in ORDERS:
         codes = [(kinds.index(kind) * depth + at) * 4 + q for kind, at, q in order]
-        codes += [idle] * (-len(codes) % per_word)
+        codes += [idle] * (longest - len(codes))
         words.append([
             sum(code * base**n for n, code in enumerate(codes[first : first + per_word]))
             for first in range(0, len(codes), per_word)
@@ -269,17 +274,20 @@
     def far_sum_up(at, h):
         return link(part.at[at, 3, core, cuts[h]], far_below.at[at, cuts[h]], 34 + h, at, above)
 
-    def home_low():
-        return link(part.at[level, 3, core, cuts[0]], home_left, 36, 0, left)
-
-    def home_high():
-        return link(part.at[level, 3, core, cuts[1]], home_right, 37, 0, right)
-
-    def last_low():
-        return link(home_left, far_back.at[cuts[0]], 38, 0, left)
-
-    def last_high():
-        return link(home_right, far_back.at[cuts[1]], 39, 0, right)
+    def home_low(at):
+        return link(part.at[at, 3, core, cuts[0]], home_left.at[at], 36, at, left)
+
+    def home_high(at):
+        return link(part.at[at, 3, core, cuts[1]], home_right.at[at], 37, at, right)
+
+    def last_low(at):
+        return link(home_left.at[at], far_back.at[at, cuts[0]], 38, at, left)
+
+    def last_high(at):
+        return link(home_right.at[at], far_back.at[at, cuts[1]], 39, at, right)
+
+    def crosses(at):
+        return (at == level) | (at - level >= depth - 1) | (level - at >= depth - 1)
 
     place = column * 2 * depth + line
     last_place = lax.axis_size("ep") * 2 * depth - 1
@@ -420,7 +428,13 @@
         pl.when(jnp.logical_not(above_too | below_too))(lambda: action(False, False))
 
     def far_total(at, h):
-        above_too, below_too = (at <= level) & has_above, (at >= level) & has_below
+        above_too = (at <= level) & has_above & (level + 1 - at < depth - 1)
+        below_too = (at >= level) & has_below & (at - level + 1 < depth - 1)
+        over = crosses(at)
+        above_too, below_too = (
+            above_too & ((at == level) | jnp.logical_not(over)),
+            below_too & ((at == level) | jnp.logical_not(over)),
+        )
         pl.when(above_too)(lambda: far_sum_down(at, h).wait_recv())
         pl.when(below_too)(lambda: far_sum_up(at, h).wait_recv())
 
@@ -436,9 +450,10 @@
             by_piece((0, low)[h], (low, high)[h], step_rows, body)
 
         with_incoming(above_too, below_too, action)
-        pl.when(at < level)(lambda: far_sum_down(at, h).start())
-        pl.when(at > level)(lambda: far_sum_up(at, h).start())
-        pl.when(at == level)(lambda: (home_low, home_high)[h]().start())
+        chained = jnp.logical_not(over)
+        pl.when(chained & (at < level))(lambda: far_sum_down(at, h).start())
+        pl.when(chained & (at > level))(lambda: far_sum_up(at, h).start())
+        pl.when(over)(lambda: (home_low, home_high)[h](at).start())
 
     def far_step(at, h):
         pl.when(h == 0)(lambda: give(at, 3).wait_recv())
@@ -470,8 +485,20 @@
         back_left(at).wait_recv()
         back_right(at).wait_recv()
         own = (part[at, 0, core].astype(f32) + from_core[at, 0].astype(f32)).astype(bf16)
-        results = jnp.concatenate([own, from_right[at], from_left[at]], axis=0)
-        local[at] = placed(at, (column, right_column, left_column), results)
+        results = [own, from_right[at], from_left[at]]
+        chosen = (column, right_column, left_column)
+        four = crosses(at) & (at != level)
+
+        @pl.when(four)
+        def _():
+            last_low(at).wait_recv()
+            last_high(at).wait_recv()
+            every = jnp.concatenate([*results, far_back[at]], axis=0)
+            local[at] = placed(at, (*chosen, far_column), every)
+
+        @pl.when(jnp.logical_not(four))
+        def _():
+            local[at] = placed(at, chosen, jnp.concatenate(results, axis=0))
 
     def arrive(at, h):
         upward, downward = (at <= level) & has_above, (at >= level) & has_below
@@ -541,18 +568,18 @@
     def home_relay(at, h):
         @pl.when(h == 0)
         def _():
-            home_low().wait_recv()
-            last_low().start()
+            home_low(at).wait_recv()
+            last_low(at).start()
 
         @pl.when(h == 1)
         def _():
-            home_high().wait_recv()
-            last_high().start()
+            home_high(at).wait_recv()
+            last_high(at).start()
 
     def finish(at, _):
-        last_low().wait_recv()
-        last_high().wait_recv()
-        total = placed(level, (far_column,), far_back[...])
+        last_low(level).wait_recv()
+        last_high(level).wait_recv()
+        total = placed(level, (far_column,), far_back[level])
         out_ref[...] = (dense[level].astype(f32) + total).astype(bf16)
 
     def mixer_rows(at, _):
@@ -605,11 +632,39 @@
         for number in range(4):
             pl.when(q == number)(functools.partial(mixer_group, number))
 
+    def settle(use, copy, *more):
+        pl.when(use)(lambda: copy(*more).wait_send())
+
+    def settle_out(at, _):
+        upward, downward = (at <= level) & has_above, (at >= level) & has_below
+        for copy in (table_up, far_up):
+            settle(upward, copy, at)
+        for copy in (table_down, far_down):
+            settle(downward, copy, at)
+        for h in range(2):
+            settle(upward, up, at, h)
+            settle(downward, down, at, h)
+        for copy in (to_right, to_left):
+            copy(at).wait_send()
+        for q in range(4):
+            share(at, q).wait_send()
+
+        @pl.when(at == level)
+        def _():
+            for copy in (far_right, far_left, on_right, on_left):
+                copy().wait_send()
+
+    def settle_back(at, _):
+        for copy in (back_left, back_right):
+            copy(at).wait_send()
+        for q in range(4):
+            give(at, q).wait_send()
+
     actions = dict(
         D=arrive, M=sides_out, I=sides_in, G=far_in,
         C=multiply, P=back, F=far_step, S=dense_step,
         E=expand, X=far_out, Y=relay, V=home_relay, Z=finish,
-        H=mixer_rows, Q=mixer_step,
+        H=mixer_rows, Q=mixer_step, K=settle_out, L=settle_back,
     )
     kinds = list(actions)
     words, per_word, base = coded_orders(depth, kinds)
@@ -643,35 +698,31 @@
     lax.fori_loop(0, len(words[0]), one_word, 0)
 
     def drain(at, carry):
-        upward, downward = (at <= level) & has_above, (at >= level) & has_below
-
-        def settle(use, copy, *more):
-            pl.when(use)(lambda: copy(at, *more).wait_send())
-
-        settle(upward, table_up)
-        settle(downward, table_down)
-        settle(upward, far_up)
-        settle(downward, far_down)
-        for h in range(2):
-            settle(upward, up, h)
-            settle(downward, down, h)
-            settle(at < level, far_sum_down, h)
-            settle(at > level, far_sum_up, h)
-        for h in range(4):
-            settle(at < level, sum_down, h)
-            settle(at > level, sum_up, h)
-        for copy in (to_right, to_left, back_left, back_right):
-            copy(at).wait_send()
-        for q in range(4):
-            share(at, q).wait_send()
-            give(at, q).wait_send()
+        over = crosses(at)
+        chained = jnp.logical_not(over)
+
+        @pl.when(at < level)
+        def _():
+            for h in range(4):
+                sum_down(at, h).wait_send()
+            for h in range(2):
+                settle(chained, far_sum_down, at, h)
+
+        @pl.when(at > level)
+        def _():
+            for h in range(4):
+                sum_up(at, h).wait_send()
+            for h in range(2):
+                settle(chained, far_sum_up, at, h)
+
+        @pl.when(over)
+        def _():
+            for copy in (home_low, home_high, last_low, last_high):
+                copy(at).wait_send()
+
         return carry
 
     lax.fori_loop(0, depth, drain, 0)
-    for copy in (
-        far_right, far_left, on_right, on_left, home_low, home_high, last_low, last_high
-    ):
-        copy().wait_send()
     pl.when(has_following)(lambda: to_following().wait_send())
     pl.when(has_preceding)(lambda: to_preceding().wait_send())
 
@@ -692,11 +743,11 @@
     vmem, anywhere = pl.BlockSpec(memory_space=pltpu.VMEM), pl.BlockSpec(memory_space=pl.ANY)
     compact = pltpu.VMEM((depth, capacity, width), bf16)
     dense = pltpu.VMEM((depth, row_count, width), bf16)
-    result = jax.ShapeDtypeStruct((row_count, width), bf16)
+    held = pltpu.VMEM((row_count, width), bf16)
     stationary = (w_gate[0], w_up[0], w_down[0], mixer_input, group_weight)
     return pl.pallas_call(
         functools.partial(stream_kernel, depth, capacity, experts),
-        out_shape=(result, result),
+        out_shape=(held, held),
         in_specs=[vmem] * 6 + [anywhere] * 5,
         out_specs=(vmem, vmem),
         scratch_shapes=[
@@ -720,9 +771,9 @@
             dense,
             compact,
             compact,
-            pltpu.VMEM((low, width), bf16),
-            pltpu.VMEM((high, width), bf16),
-            pltpu.VMEM((capacity, width), bf16),
+            pltpu.VMEM((depth, low, width), bf16),
+            pltpu.VMEM((depth, high, width), bf16),
+            compact,
             pltpu.SemaphoreType.DMA((42, depth)),
             pltpu.SemaphoreType.DMA((42, depth)),
             pltpu.SemaphoreType.DMA((len(stationary),)),

time: 97.2 us -> 93.2 us (0.959)
  Pallas kernels: 93.8 us -> 90.9 us
  local copies, waits for them, and re-layouts: 2.57 us -> 1.49 us
    pallas_call x1, Pallas kernels: 93.8 us -> 90.9 us  [dense_plan(): pl.pallas_call(functools.partial(stream_kernel, depth, capacity, experts)...]
    unnamed x4 -> x2, local copies, waits for them, and re-layouts: 2.57 us -> 1.49 us
where the time goes in v4:
time: 93.2 us; the launch traced here: 93 us
  Pallas kernels  90.9 us (98%)
  local copies, waits for them, and re-layouts  1.49 us (2%)
    pallas_call x1, Pallas kernels, dense_plan(): pl.pallas_call(functools.partial(stream_kernel, depth, capacity, experts)...  90.9 us

profile of v4, /device:TPU:0, one launch (start us, length us, event | category | flops | bytes accessed | tf_op | source)
XLA Modules:
  0.0 93.0 jit_solution(801234065603099884)
XLA Ops:
  0.6 90.9 %shard_map.122 = (bf16[192,1024]{1,0:T(8,128)(2,1)S(1)}, bf16[192,1024]{1,0:T(8,128)(2,1)S(1)}) custom-call(bf16[192,1024]{1,0:T(8,128)(2,1)} %input_ref.1, f32[1,1024]{1,0:T(1,128)} %bitcast.11, s32[2,192]{1,0:T(2,128)} %bitcast.14, f32[2,192]{1,0:T(2,128)} %bitcast.15, f32[1,1024]{1,0:T(1,128)} %bitcast.12, f32[1,1024]{1,0:T(1,128)} %bitcast.13, ...), custom_call_target="tpu_custom_call" | custom-call | tf_op jit(solution)/shard_map/pallas_call | solution.py:748
  91.5 0.7 copy.15
  92.3 0.7 copy.16

commit v5 on v4

--- a/solution.py
+++ b/solution.py
@@ -119,35 +119,35 @@
 
 ORDERS = (
     (
-        ("D", 0, 1), ("D", 0, 0), ("X", 0, 0), ("Y", 0, 0), ("M", 0, 0), ("C", 0, 0), ("D", 1, 1),
-        ("D", 1, 0), ("M", 1, 0), ("G", 0, 0), ("C", 0, 3), ("I", 0, 0), ("D", 2, 0), ("D", 2, 1),
-        ("M", 2, 0), ("C", 0, 2), ("I", 1, 0), ("C", 2, 0), ("C", 1, 0), ("K", 0, 0), ("D", 3, 0),
-        ("D", 3, 1), ("M", 3, 0), ("C", 0, 1), ("I", 2, 0), ("C", 1, 2), ("C", 2, 1), ("G", 1, 0),
-        ("C", 2, 2), ("P", 2, 1), ("C", 1, 3), ("P", 2, 2), ("I", 3, 0), ("K", 1, 0), ("C", 1, 1),
-        ("F", 1, 0), ("G", 3, 0), ("F", 1, 1), ("C", 3, 2), ("C", 3, 3), ("C", 3, 1), ("F", 3, 0),
-        ("F", 3, 1), ("K", 3, 0), ("E", 2, 0), ("S", 2, 1), ("G", 2, 0), ("P", 3, 1), ("S", 2, 2),
-        ("S", 2, 0), ("P", 3, 2), ("C", 2, 3), ("F", 2, 0), ("K", 2, 0), ("V", 3, 0), ("P", 1, 1),
-        ("C", 3, 0), ("V", 3, 1), ("P", 1, 2), ("F", 2, 1), ("L", 2, 0), ("F", 0, 0), ("S", 2, 3),
-        ("H", 0, 0), ("P", 0, 2), ("E", 3, 0), ("S", 3, 0), ("S", 3, 2), ("Q", 0, 0), ("F", 0, 1),
-        ("S", 3, 1), ("L", 3, 0), ("S", 3, 3), ("Q", 0, 1), ("P", 0, 1), ("E", 1, 0), ("S", 1, 1),
-        ("S", 1, 2), ("L", 1, 0), ("S", 1, 0), ("Q", 0, 3), ("S", 1, 3), ("Q", 0, 2), ("V", 0, 0),
-        ("V", 0, 1), ("E", 0, 0), ("S", 0, 1), ("L", 0, 0), ("S", 0, 2), ("S", 0, 0), ("S", 0, 3),
+        ("D", 0, 1), ("D", 0, 0), ("X", 0, 0), ("M", 0, 0), ("Y", 0, 0), ("D", 1, 0), ("D", 1, 1),
+        ("M", 1, 0), ("I", 0, 0), ("C", 1, 0), ("G", 0, 0), ("C", 0, 2), ("C", 0, 1), ("D", 2, 0),
+        ("D", 2, 1), ("M", 2, 0), ("I", 1, 0), ("K", 0, 0), ("C", 1, 1), ("D", 3, 1), ("C", 2, 0),
+        ("D", 3, 0), ("M", 3, 0), ("I", 2, 0), ("C", 1, 2), ("C", 2, 1), ("C", 2, 2), ("C", 0, 3),
+        ("G", 1, 0), ("P", 2, 2), ("P", 2, 1), ("I", 3, 0), ("C", 1, 3), ("C", 3, 1), ("F", 1, 0),
+        ("C", 3, 2), ("F", 1, 1), ("P", 3, 1), ("K", 1, 0), ("G", 3, 0), ("C", 0, 0), ("P", 3, 2),
+        ("C", 3, 3), ("E", 2, 0), ("S", 2, 3), ("C", 3, 0), ("S", 2, 2), ("S", 2, 1), ("G", 2, 0),
+        ("F", 3, 0), ("F", 3, 1), ("C", 2, 3), ("F", 2, 0), ("K", 3, 0), ("V", 3, 0), ("K", 2, 0),
+        ("L", 3, 0), ("V", 3, 1), ("P", 1, 2), ("F", 2, 1), ("H", 0, 0), ("S", 2, 0), ("P", 1, 1),
+        ("F", 0, 0), ("E", 3, 0), ("S", 3, 1), ("S", 3, 3), ("S", 3, 2), ("F", 0, 1), ("S", 3, 0),
+        ("Q", 0, 0), ("P", 0, 2), ("Q", 0, 3), ("E", 1, 0), ("S", 1, 1), ("P", 0, 1), ("V", 0, 1),
+        ("S", 1, 3), ("L", 2, 0), ("L", 1, 0), ("S", 1, 0), ("V", 0, 0), ("Q", 0, 2), ("Q", 0, 1),
+        ("S", 1, 2), ("E", 0, 0), ("S", 0, 1), ("S", 0, 3), ("S", 0, 2), ("L", 0, 0), ("S", 0, 0),
         ("Z", 0, 0),
     ),
     (
-        ("D", 1, 0), ("D", 1, 1), ("X", 1, 0), ("M", 1, 0), ("D", 0, 1), ("D", 2, 0), ("Y", 1, 0),
-        ("D", 2, 1), ("M", 2, 0), ("D", 0, 0), ("C", 1, 0), ("I", 1, 0), ("D", 3, 1), ("C", 1, 1),
-        ("M", 0, 0), ("C", 1, 2), ("D", 3, 0), ("C", 2, 0), ("M", 3, 0), ("G", 0, 0), ("C", 0, 0),
-        ("I", 2, 0), ("G", 1, 0), ("P", 1, 2), ("P", 1, 1), ("C", 2, 1), ("C", 0, 3), ("I", 0, 0),
-        ("C", 2, 2), ("G", 3, 0), ("C", 0, 1), ("C", 0, 2), ("C", 3, 3), ("K", 0, 0), ("P", 2, 1),
-        ("C", 3, 0), ("G", 2, 0), ("F", 3, 0), ("I", 3, 0), ("C", 1, 3), ("F", 3, 1), ("C", 2, 3),
-        ("P", 2, 2), ("C", 3, 1), ("C", 3, 2), ("P", 0, 1), ("K", 1, 0), ("H", 1, 0), ("E", 1, 0),
-        ("K", 2, 0), ("F", 0, 0), ("K", 3, 0), ("P", 3, 1), ("P", 3, 2), ("P", 0, 2), ("E", 2, 0),
-        ("L", 2, 0), ("F", 0, 1), ("S", 2, 1), ("L", 1, 0), ("S", 2, 0), ("S", 2, 2), ("F", 2, 0),
-        ("Q", 1, 0), ("F", 2, 1), ("E", 0, 0), ("E", 3, 0), ("S", 3, 0), ("F", 1, 0), ("Q", 1, 1),
-        ("S", 3, 2), ("F", 1, 1), ("L", 0, 0), ("L", 3, 0), ("Q", 1, 3), ("S", 3, 1), ("S", 0, 0),
-        ("Q", 1, 2), ("S", 3, 3), ("S", 0, 2), ("S", 2, 3), ("S", 0, 1), ("V", 1, 1), ("V", 1, 0),
-        ("S", 0, 3), ("S", 1, 0), ("S", 1, 2), ("S", 1, 3), ("S", 1, 1), ("Z", 1, 0),
+        ("D", 1, 0), ("D", 1, 1), ("X", 1, 0), ("M", 1, 0), ("D", 0, 1), ("C", 1, 0), ("Y", 1, 0),
+        ("D", 2, 0), ("D", 0, 0), ("D", 2, 1), ("M", 2, 0), ("M", 0, 0), ("I", 1, 0), ("D", 3, 1),
+        ("C", 1, 1), ("C", 1, 2), ("D", 3, 0), ("C", 2, 0), ("M", 3, 0), ("P", 1, 2), ("I", 2, 0),
+        ("C", 3, 0), ("G", 0, 0), ("P", 1, 1), ("C", 2, 2), ("G", 1, 0), ("C", 2, 1), ("I", 0, 0),
+        ("C", 0, 0), ("C", 0, 2), ("G", 3, 0), ("C", 0, 1), ("P", 2, 2), ("I", 3, 0), ("C", 3, 3),
+        ("C", 0, 3), ("P", 0, 2), ("C", 3, 2), ("G", 2, 0), ("F", 3, 0), ("P", 2, 1), ("F", 3, 1),
+        ("P", 0, 1), ("C", 3, 1), ("P", 3, 1), ("K", 1, 0), ("C", 1, 3), ("L", 1, 0), ("C", 2, 3),
+        ("K", 3, 0), ("F", 0, 0), ("E", 1, 0), ("F", 0, 1), ("K", 2, 0), ("E", 2, 0), ("H", 1, 0),
+        ("S", 2, 3), ("L", 2, 0), ("P", 3, 2), ("S", 2, 1), ("S", 2, 2), ("F", 2, 0), ("F", 2, 1),
+        ("E", 3, 0), ("L", 0, 0), ("Q", 1, 0), ("E", 0, 0), ("K", 0, 0), ("F", 1, 0), ("L", 3, 0),
+        ("S", 3, 1), ("Q", 1, 2), ("Q", 1, 1), ("F", 1, 1), ("S", 3, 3), ("S", 3, 2), ("S", 0, 1),
+        ("V", 1, 0), ("S", 3, 0), ("S", 0, 3), ("S", 0, 2), ("S", 1, 1), ("S", 2, 0), ("V", 1, 1),
+        ("Q", 1, 3), ("S", 0, 0), ("S", 1, 3), ("S", 1, 0), ("S", 1, 2), ("Z", 1, 0),
     ),
 )
 
@@ -171,15 +171,42 @@
     return words, per_word, base
 
 
+def slot_tables(depth):
+    def offsets(**sizes):
+        table, count = {}, 0
+        for name, size in sizes.items():
+            table[name], count = count, count + size
+        return dict(table, count=count)
+
+    sends = offsets(
+        rows=depth + 1, table=depth + 1, farther=depth + 1, sides=depth, share=depth,
+        give=depth, back=depth, sum=depth, farsum=depth, far=1, on=1, home=2, last=2, halo=2,
+    )
+    receives = offsets(
+        rows=2 * depth, table=depth, farther=depth, sides=depth, share=4 * depth,
+        give=4 * depth, back=depth, sum=4 * depth + 4, farsum=2 * depth + 2,
+        far=1, on=1, home=4, last=2, halo=2,
+    )
+    return sends, receives
+
+
 def stream_kernel(
-    depth, capacity, experts,
-    input_ref, gain_ref, routes_ref, weight_ref, mixer_gain_ref, mixer_scale_ref,
-    gate_hbm, up_hbm, down_hbm, mixer_hbm, group_hbm, mixed_ref, out_ref,
-    gate_ref, up_ref, down_ref, mixer_ref, group_ref, mix, tok, tables, blk, part, from_core, out_right, out_left, out_far, relay_right, relay_left,
-    from_right, from_left, local, dense, dense_above, dense_below,
-    far_above, far_below, home_left, home_right, far_back,
-    send_sem, recv_sem, local_sem,
+    depth, capacity, experts, stores,
+    *refs,
 ):
+    stored, refs = refs[:stores], refs[stores:]
+    mixed_ref, out_ref, *refs = refs
+    held, refs = refs[:stores], refs[stores:]
+    (
+        input_ref, gain_ref, routes_ref, weight_ref, gate_ref, up_ref, down_ref,
+        mixer_ref, group_ref, mixer_gain_ref, mixer_scale_ref,
+    ) = held
+    (
+        mix, tok, tables, blk, part, from_core, sides, out_far, passing,
+        from_sides, local, dense, dense_above, dense_below,
+        far_above, far_below, home, far_back,
+        send_sem, recv_sem, local_sem,
+    ) = refs
     column, line = lax.axis_index("ep"), lax.axis_index("tp")
     level, core = line // 2, line % 2
     other = 1 - core
@@ -196,95 +223,178 @@
     has_above, has_below = level < depth - 1, level > 0
     f32, bf16 = jnp.float32, jnp.bfloat16
 
-    def link(src, dst, kind, at, target):
+    def link(src, dst, sent, got, target):
         return pltpu.make_async_remote_copy(
-            src_ref=src, dst_ref=dst, send_sem=send_sem.at[kind, at],
-            recv_sem=recv_sem.at[kind, at], device_id=target,
+            src_ref=src, dst_ref=dst, send_sem=send_sem.at[sent],
+            recv_sem=recv_sem.at[got], device_id=target,
             device_id_type=pl.DeviceIdType.MESH,
         )
 
+    sends, receives = slot_tables(depth)
+
+    def twin(at, where):
+        return jnp.where(at == where, depth, at)
+
     def part_of(h):
         return pl.ds(pl.multiple_of(h * half, half), half)
 
-    def up(at, h):
-        return link(tok.at[at, part_of(h)], tok.at[at, part_of(h)], h, at, above)
-
-    def down(at, h):
-        return link(tok.at[at, part_of(h)], tok.at[at, part_of(h)], 2 + h, at, below)
-
-    def table_up(at):
-        return link(tables.at[at], tables.at[at], 4, at, above)
-
-    def table_down(at):
-        return link(tables.at[at], tables.at[at], 5, at, below)
-
-    def to_right(at):
-        return link(out_right.at[at], blk.at[at, 1, core], 6, at, right)
-
-    def to_left(at):
-        return link(out_left.at[at], blk.at[at, 2, core], 7, at, left)
-
-    def far_right():
-        return link(out_far.at[pl.ds(0, low)], relay_right, 8, 0, right)
-
-    def far_left():
-        return link(out_far.at[pl.ds(low, high)], relay_left, 9, 0, left)
-
-    def on_right():
-        return link(relay_right, blk.at[level, 3, core, pl.ds(0, low)], 10, 0, right)
-
-    def on_left():
-        return link(relay_left, blk.at[level, 3, core, pl.ds(low, high)], 11, 0, left)
-
-    def far_up(at):
-        return link(blk.at[at, 3, core], blk.at[at, 3, core], 12, at, above)
-
-    def far_down(at):
-        return link(blk.at[at, 3, core], blk.at[at, 3, core], 13, at, below)
-
-    def share(at, q):
-        return link(blk.at[at, q, core], blk.at[at, q, core], 14 + q, at, beside)
-
-    def shared_in(at, q):
-        return link(blk.at[at, q, other], blk.at[at, q, other], 14 + q, at, beside)
-
-    def give(at, q):
-        return link(part.at[at, q, other], from_core.at[at, q], 18 + q, at, beside)
-
-    def back_left(at):
-        return link(part.at[at, 1, core], from_right.at[at], 22, at, left)
-
-    def back_right(at):
-        return link(part.at[at, 2, core], from_left.at[at], 23, at, right)
-
     def fourth(h):
         return pl.ds(pl.multiple_of(h * quarter, quarter), quarter)
 
+    cuts = (pl.ds(0, low), pl.ds(low, high))
+
+    def up(at, h):
+        span = tok.at[at, part_of(h)]
+        return link(span, span, sends["rows"] + at, receives["rows"] + 2 * at + h, above)
+
+    def down(at, h):
+        span, sent = tok.at[at, part_of(h)], sends["rows"] + twin(at, level)
+        return link(span, span, sent, receives["rows"] + 2 * at + h, below)
+
+    def all_up(at):
+        return link(tok.at[at], tok.at[at], sends["rows"] + at, receives["rows"], above)
+
+    def all_down(at):
+        sent = sends["rows"] + twin(at, level)
+        return link(tok.at[at], tok.at[at], sent, receives["rows"], below)
+
+    def table_up(at):
+        table = tables.at[at]
+        return link(table, table, sends["table"] + at, receives["table"] + at, above)
+
+    def table_down(at):
+        table, sent = tables.at[at], sends["table"] + twin(at, level)
+        return link(table, table, sent, receives["table"] + at, below)
+
+    def to_right(at):
+        sent, got = sends["sides"] + at, receives["sides"] + at
+        return link(sides.at[at, 0], blk.at[at, 1, core], sent, got, right)
+
+    def to_left(at):
+        sent, got = sends["sides"] + at, receives["sides"] + at
+        return link(sides.at[at, 1], blk.at[at, 2, core], sent, got, left)
+
+    def all_sides(at):
+        sent, got = sends["sides"] + at, receives["sides"] + at
+        return link(sides.at[at], blk.at[at, pl.ds(1, 2), core], sent, got, right)
+
+    def far_right():
+        span = cuts[0]
+        return link(out_far.at[span], passing.at[span], sends["far"], receives["far"], right)
+
+    def far_left():
+        span = cuts[1]
+        return link(out_far.at[span], passing.at[span], sends["far"], receives["far"], left)
+
+    def all_far():
+        return link(out_far, passing, sends["far"], receives["far"], right)
+
+    def on_right():
+        there = blk.at[level, 3, core, cuts[0]]
+        return link(passing.at[cuts[0]], there, sends["on"], receives["on"], right)
+
+    def on_left():
+        there = blk.at[level, 3, core, cuts[1]]
+        return link(passing.at[cuts[1]], there, sends["on"], receives["on"], left)
+
+    def all_on():
+        return link(passing, blk.at[level, 3, core], sends["on"], receives["on"], right)
+
+    def far_up(at):
+        block = blk.at[at, 3, core]
+        return link(block, block, sends["farther"] + at, receives["farther"] + at, above)
+
+    def far_down(at):
+        block, sent = blk.at[at, 3, core], sends["farther"] + twin(at, level)
+        return link(block, block, sent, receives["farther"] + at, below)
+
+    def share(at, q):
+        block = blk.at[at, q, core]
+        return link(block, block, sends["share"] + at, receives["share"] + 4 * at + q, beside)
+
+    def shared_in(at, q):
+        block = blk.at[at, q, other]
+        return link(block, block, sends["share"] + at, receives["share"] + 4 * at + q, beside)
+
+    def all_shared(at):
+        blocks = blk.at[at, pl.ds(0, 4), core]
+        return link(blocks, blocks, sends["share"] + at, receives["share"], beside)
+
+    def give(at, q):
+        sent, got = sends["give"] + at, receives["give"] + 4 * at + q
+        return link(part.at[at, q, other], from_core.at[at, q], sent, got, beside)
+
+    def all_given(at):
+        given = part.at[at, pl.ds(0, 4), other]
+        return link(given, from_core.at[at], sends["give"] + at, receives["give"], beside)
+
+    def back_left(at):
+        sent, got = sends["back"] + at, receives["back"] + at
+        return link(part.at[at, 1, core], from_sides.at[at, 0], sent, got, left)
+
+    def back_right(at):
+        sent, got = sends["back"] + at, receives["back"] + at
+        return link(part.at[at, 2, core], from_sides.at[at, 1], sent, got, right)
+
+    def all_back(at):
+        sent, got = sends["back"] + at, receives["back"] + at
+        return link(part.at[at, pl.ds(1, 2), core], from_sides.at[at], sent, got, left)
+
     def sum_down(at, h):
-        return link(dense.at[at, fourth(h)], dense_above.at[at, fourth(h)], 24 + h, at, below)
-
-    def sum_up(at, h):
-        return link(dense.at[at, fourth(h)], dense_below.at[at, fourth(h)], 28 + h, at, above)
-
-    cuts = (pl.ds(0, low), pl.ds(low, high))
+        span, got = fourth(h), receives["sum"] + 4 * at + h
+        return link(dense.at[at, span], dense_above.at[at, span], sends["sum"] + at, got, below)
+
+    def sum_up(at, h, receiver):
+        span, got = fourth(h), receives["sum"] + 4 * twin(at, receiver) + h
+        return link(dense.at[at, span], dense_below.at[at, span], sends["sum"] + at, got, above)
+
+    def all_summed(at):
+        sent = sends["sum"] + at
+        return link(dense.at[at], dense_above.at[at], sent, receives["sum"], below)
 
     def far_sum_down(at, h):
-        return link(part.at[at, 3, core, cuts[h]], far_above.at[at, cuts[h]], 32 + h, at, below)
-
-    def far_sum_up(at, h):
-        return link(part.at[at, 3, core, cuts[h]], far_below.at[at, cuts[h]], 34 + h, at, above)
+        span, sent, got = cuts[h], sends["farsum"] + at, receives["farsum"] + 2 * at + h
+        return link(part.at[at, 3, core, span], far_above.at[at, span], sent, got, below)
+
+    def far_sum_up(at, h, receiver):
+        span, sent = cuts[h], sends["farsum"] + at
+        got = receives["farsum"] + 2 * twin(at, receiver) + h
+        return link(part.at[at, 3, core, span], far_below.at[at, span], sent, got, above)
+
+    def all_far_summed(at):
+        sent = sends["farsum"] + at
+        return link(part.at[at, 3, core], far_above.at[at], sent, receives["farsum"], below)
+
+    def pocket(at):
+        return jnp.where(at == level, 0, 1)
 
     def home_low(at):
-        return link(part.at[at, 3, core, cuts[0]], home_left.at[at], 36, at, left)
+        n, span = pocket(at), cuts[0]
+        sent, got = sends["home"] + n, receives["home"] + 2 * n
+        return link(part.at[at, 3, core, span], home.at[n, span], sent, got, left)
 
     def home_high(at):
-        return link(part.at[at, 3, core, cuts[1]], home_right.at[at], 37, at, right)
+        n, span = pocket(at), cuts[1]
+        sent, got = sends["home"] + n, receives["home"] + 2 * n + 1
+        return link(part.at[at, 3, core, span], home.at[n, span], sent, got, right)
+
+    def all_home(at):
+        n = pocket(at)
+        return link(part.at[at, 3, core], home.at[n], sends["home"] + n, receives["home"], left)
 
     def last_low(at):
-        return link(home_left.at[at], far_back.at[at, cuts[0]], 38, at, left)
+        n, span = pocket(at), cuts[0]
+        sent, got = sends["last"] + n, receives["last"] + n
+        return link(home.at[n, span], far_back.at[n, span], sent, got, left)
 
     def last_high(at):
-        return link(home_right.at[at], far_back.at[at, cuts[1]], 39, at, right)
+        n, span = pocket(at), cuts[1]
+        sent, got = sends["last"] + n, receives["last"] + n
+        return link(home.at[n, span], far_back.at[n, span], sent, got, right)
+
+    def all_last(at):
+        n = pocket(at)
+        return link(home.at[n], far_back.at[n], sends["last"] + n, receives["last"] + n, left)
 
     def crosses(at):
         return (at == level) | (at - level >= depth - 1) | (level - at >= depth - 1)
@@ -296,20 +406,19 @@
     preceding = (column - jnp.where(first_line, 1, 0), jnp.where(first_line, 2 * depth - 1, line - 1))
     has_following, has_preceding = place < last_place, place > 0
 
+    halo, halo_in = sends["halo"], receives["halo"]
+
     def to_following():
-        return link(mix.at[pl.ds(rows, edge)], mix.at[pl.ds(0, edge)], 40, 0, following)
+        return link(mix.at[pl.ds(rows, edge)], mix.at[pl.ds(0, edge)], halo, halo_in, following)
 
     def to_preceding():
         return link(
-            mix.at[pl.ds(edge, edge)], mix.at[pl.ds(edge + rows, edge)], 41, 0, preceding
+            mix.at[pl.ds(edge, edge)], mix.at[pl.ds(edge + rows, edge)], halo + 1, halo_in + 1, preceding
         )
 
     loads = [
         pltpu.make_async_copy(src, dst, local_sem.at[n])
-        for n, (src, dst) in enumerate((
-            (gate_hbm, gate_ref), (up_hbm, up_ref), (down_hbm, down_ref),
-            (mixer_hbm, mixer_ref), (group_hbm, group_ref),
-        ))
+        for n, (src, dst) in enumerate(zip(stored, held))
     ]
     def by_piece(start, count, width, body):
         def one(i, carry):
@@ -332,6 +441,8 @@
     pl.when(has_below)(lambda: greet(below))
     for load in loads:
         load.start()
+    for load in loads[:4]:
+        load.wait()
 
     def normed(values, gains):
         values = values.astype(f32)
@@ -436,7 +547,7 @@
             below_too & ((at == level) | jnp.logical_not(over)),
         )
         pl.when(above_too)(lambda: far_sum_down(at, h).wait_recv())
-        pl.when(below_too)(lambda: far_sum_up(at, h).wait_recv())
+        pl.when(below_too)(lambda: far_sum_up(at, h, level).wait_recv())
 
         def action(from_up, from_down):
             def body(span):
@@ -452,7 +563,7 @@
         with_incoming(above_too, below_too, action)
         chained = jnp.logical_not(over)
         pl.when(chained & (at < level))(lambda: far_sum_down(at, h).start())
-        pl.when(chained & (at > level))(lambda: far_sum_up(at, h).start())
+        pl.when(chained & (at > level))(lambda: far_sum_up(at, h, level + 1).start())
         pl.when(over)(lambda: (home_low, home_high)[h](at).start())
 
     def far_step(at, h):
@@ -463,7 +574,7 @@
     def dense_step(at, h):
         above_too, below_too = (at <= level) & has_above, (at >= level) & has_below
         pl.when(above_too)(lambda: sum_down(at, h).wait_recv())
-        pl.when(below_too)(lambda: sum_up(at, h).wait_recv())
+        pl.when(below_too)(lambda: sum_up(at, h, level).wait_recv())
 
         def action(from_up, from_down):
             def body(span):
@@ -478,22 +589,20 @@
 
         with_incoming(above_too, below_too, action)
         pl.when(at < level)(lambda: sum_down(at, h).start())
-        pl.when(at > level)(lambda: sum_up(at, h).start())
+        pl.when(at > level)(lambda: sum_up(at, h, level + 1).start())
 
     def expand(at, _):
         give(at, 0).wait_recv()
-        back_left(at).wait_recv()
-        back_right(at).wait_recv()
+        all_back(at).wait_recv()
         own = (part[at, 0, core].astype(f32) + from_core[at, 0].astype(f32)).astype(bf16)
-        results = [own, from_right[at], from_left[at]]
+        results = [own, from_sides[at, 0], from_sides[at, 1]]
         chosen = (column, right_column, left_column)
         four = crosses(at) & (at != level)
 
         @pl.when(four)
         def _():
-            last_low(at).wait_recv()
-            last_high(at).wait_recv()
-            every = jnp.concatenate([*results, far_back[at]], axis=0)
+            all_last(at).wait_recv()
+            every = jnp.concatenate([*results, far_back[1]], axis=0)
             local[at] = placed(at, (*chosen, far_column), every)
 
         @pl.when(jnp.logical_not(four))
@@ -519,36 +628,30 @@
         out_far[...] = picked(at, (far_column,))
         far_right().start()
         far_left().start()
-        for load in loads[:3]:
+        for load in loads[4:7]:
             load.wait()
 
     def relay(at, _):
-        far_right().wait_recv()
+        all_far().wait_recv()
         on_right().start()
-        far_left().wait_recv()
         on_left().start()
 
     def sides_out(at, _):
         sent = picked(at, (right_column, left_column, column))
-        out_right[at] = sent[:capacity]
-        out_left[at] = sent[capacity : 2 * capacity]
+        sides[at, 0] = sent[:capacity]
+        sides[at, 1] = sent[capacity : 2 * capacity]
         to_right(at).start()
         to_left(at).start()
         blk[at, 0, core] = sent[2 * capacity :]
         share(at, 0).start()
 
     def sides_in(at, _):
-        to_right(at).wait_recv()
+        all_sides(at).wait_recv()
         share(at, 1).start()
-        to_left(at).wait_recv()
         share(at, 2).start()
 
     def far_in(at, _):
-        @pl.when(at == level)
-        def _():
-            on_right().wait_recv()
-            on_left().wait_recv()
-
+        pl.when(at == level)(lambda: all_on().wait_recv())
         pl.when(at < level)(lambda: far_up(at).wait_recv())
         pl.when(at > level)(lambda: far_down(at).wait_recv())
         pl.when((at <= level) & has_above)(lambda: far_up(at).start())
@@ -577,13 +680,12 @@
             last_high(at).start()
 
     def finish(at, _):
-        last_low(level).wait_recv()
-        last_high(level).wait_recv()
-        total = placed(level, (far_column,), far_back[level])
+        all_last(level).wait_recv()
+        total = placed(level, (far_column,), far_back[0])
         out_ref[...] = (dense[level].astype(f32) + total).astype(bf16)
 
     def mixer_rows(at, _):
-        for load in loads[3:]:
+        for load in loads[7:]:
             load.wait()
 
         def body(i, carry):
@@ -637,28 +739,21 @@
 
     def settle_out(at, _):
         upward, downward = (at <= level) & has_above, (at >= level) & has_below
-        for copy in (table_up, far_up):
+        for copy in (table_up, far_up, all_up):
             settle(upward, copy, at)
-        for copy in (table_down, far_down):
+        for copy in (table_down, far_down, all_down):
             settle(downward, copy, at)
-        for h in range(2):
-            settle(upward, up, at, h)
-            settle(downward, down, at, h)
-        for copy in (to_right, to_left):
-            copy(at).wait_send()
-        for q in range(4):
-            share(at, q).wait_send()
+        all_sides(at).wait_send()
+        all_shared(at).wait_send()
 
         @pl.when(at == level)
         def _():
-            for copy in (far_right, far_left, on_right, on_left):
-                copy().wait_send()
+            all_far().wait_send()
+            all_on().wait_send()
 
     def settle_back(at, _):
-        for copy in (back_left, back_right):
-            copy(at).wait_send()
-        for q in range(4):
-            give(at, q).wait_send()
+        all_back(at).wait_send()
+        all_given(at).wait_send()
 
     actions = dict(
         D=arrive, M=sides_out, I=sides_in, G=far_in,
@@ -699,27 +794,10 @@
 
     def drain(at, carry):
         over = crosses(at)
-        chained = jnp.logical_not(over)
-
-        @pl.when(at < level)
-        def _():
-            for h in range(4):
-                sum_down(at, h).wait_send()
-            for h in range(2):
-                settle(chained, far_sum_down, at, h)
-
-        @pl.when(at > level)
-        def _():
-            for h in range(4):
-                sum_up(at, h).wait_send()
-            for h in range(2):
-                settle(chained, far_sum_up, at, h)
-
-        @pl.when(over)
-        def _():
-            for copy in (home_low, home_high, last_low, last_high):
-                copy(at).wait_send()
-
+        settle(at != level, all_summed, at)
+        settle(jnp.logical_not(over), all_far_summed, at)
+        settle(over, all_home, at)
+        settle(over, all_last, at)
         return carry
 
     lax.fori_loop(0, depth, drain, 0)
@@ -738,53 +816,49 @@
     pad = -(-3 * experts // 16) * 16
     lanes = -(-row_count // 128) * 128
     bf16, f32 = jnp.bfloat16, jnp.float32
-    low = -(-capacity // 32) * 16
-    high = capacity - low
+    sends, receives = slot_tables(depth)
     vmem, anywhere = pl.BlockSpec(memory_space=pltpu.VMEM), pl.BlockSpec(memory_space=pl.ANY)
     compact = pltpu.VMEM((depth, capacity, width), bf16)
     dense = pltpu.VMEM((depth, row_count, width), bf16)
     held = pltpu.VMEM((row_count, width), bf16)
-    stationary = (w_gate[0], w_up[0], w_down[0], mixer_input, group_weight)
+    stored = (
+        expert_input, expert_gain.reshape(1, -1), routes.T, route_weight.T,
+        w_gate[0], w_up[0], w_down[0], mixer_input, group_weight,
+        mixer_gain.reshape(1, -1), mixer_scale.reshape(1, -1),
+    )
     return pl.pallas_call(
-        functools.partial(stream_kernel, depth, capacity, experts),
+        functools.partial(stream_kernel, depth, capacity, experts, len(stored)),
         out_shape=(held, held),
-        in_specs=[vmem] * 6 + [anywhere] * 5,
+        in_specs=[anywhere] * len(stored),
         out_specs=(vmem, vmem),
         scratch_shapes=[
-            *(pltpu.VMEM(array.shape, bf16) for array in stationary),
+            *(pltpu.VMEM(array.shape, array.dtype) for array in stored),
             pltpu.VMEM((row_count + 2 * edge, width), f32),
             dense,
             pltpu.VMEM((depth, pad, lanes), bf16),
             pltpu.VMEM((depth, 4, 2, capacity, width), bf16),
             pltpu.VMEM((depth, 4, 2, capacity, width), bf16),
             pltpu.VMEM((depth, 4, capacity, width), bf16),
-            compact,
-            compact,
+            pltpu.VMEM((depth, 2, capacity, width), bf16),
             pltpu.VMEM((capacity, width), bf16),
-            pltpu.VMEM((low, width), bf16),
-            pltpu.VMEM((high, width), bf16),
-            compact,
-            compact,
+            pltpu.VMEM((capacity, width), bf16),
+            pltpu.VMEM((depth, 2, capacity, width), bf16),
             pltpu.VMEM((depth, row_count, width), f32),
             dense,
             dense,
             dense,
             compact,
             compact,
-            pltpu.VMEM((depth, low, width), bf16),
-            pltpu.VMEM((depth, high, width), bf16),
-            compact,
-            pltpu.SemaphoreType.DMA((42, depth)),
-            pltpu.SemaphoreType.DMA((42, depth)),
-            pltpu.SemaphoreType.DMA((len(stationary),)),
+            pltpu.VMEM((2, capacity, width), bf16),
+            pltpu.VMEM((2, capacity, width), bf16),
+            pltpu.SemaphoreType.DMA((sends["count"],)),
+            pltpu.SemaphoreType.DMA((receives["count"],)),
+            pltpu.SemaphoreType.DMA((len(stored),)),
         ],
         compiler_params=pltpu.CompilerParams(
             collective_id=0, has_side_effects=True, vmem_limit_bytes=60 * 2**20
         ),
-    )(
-        expert_input, expert_gain.reshape(1, -1), routes.T, route_weight.T,
-        mixer_gain.reshape(1, -1), mixer_scale.reshape(1, -1), *stationary,
-    )
+    )(*stored)
 
 
 def on_device(

time: 93.2 us -> 89 us (0.955)
  Pallas kernels: 90.9 us -> 86.7 us
    pallas_call x1, Pallas kernels: 90.9 us -> 86.7 us  [dense_plan(): pl.pallas_call(functools.partial(stream_kernel, depth, capacity, experts,...]
where the time goes in v5:
time: 89 us; the launch traced here: 88.8 us
  Pallas kernels  86.7 us (97%)
  local copies, waits for them, and re-layouts  1.49 us (2%)
    pallas_call x1, Pallas kernels, dense_plan(): pl.pallas_call(functools.partial(stream_kernel, depth, capacity, experts,...  86.7 us

profile of v5, /device:TPU:0, one launch (start us, length us, event | category | flops | bytes accessed | tf_op | source)
XLA Modules:
  0.0 88.8 jit_solution(17930902070852059949)
XLA Ops:
  0.6 86.7 %shard_map.122 = (bf16[192,1024]{1,0:T(8,128)(2,1)S(1)}, bf16[192,1024]{1,0:T(8,128)(2,1)S(1)}) custom-call(bf16[192,1024]{1,0:T(8,128)(2,1)} %refs_0_.1, f32[1,1024]{1,0:T(1,128)} %bitcast.11, s32[2,192]{1,0:T(2,128)} %bitcast.14, f32[2,192]{1,0:T(2,128)} %bitcast.15, bf16[1024,512]{1,0:T(8,128)(2,1)} %bitcast.8, bf16[1024,512]{1,0:T(8,128)(2,1)} %bitcast.9, ...), custom_call_target="tpu_custom_call" | custom-call | tf_op jit(solution)/shard_map/pallas_call | solution.py:829
  87.3 0.7 copy.15
  88.1 0.7 copy.16

commit v6 on v5

--- a/solution.py
+++ b/solution.py
@@ -153,7 +153,8 @@
 
 
 def coded_orders(depth, kinds):
-    base = len(kinds) * 4 * depth + 1
+    depth_bits = (depth - 1).bit_length()
+    base = 1 << (len(kinds) << (2 + depth_bits)).bit_length()
     per_word = 1
     while base ** (per_word + 1) < 2**31:
         per_word += 1
@@ -162,7 +163,7 @@
     longest += -longest % per_word
     words = []
     for order in ORDERS:
-        codes = [(kinds.index(kind) * depth + at) * 4 + q for kind, at, q in order]
+        codes = [((kinds.index(kind) << depth_bits) + at) * 4 + q for kind, at, q in order]
         codes += [idle] * (longest - len(codes))
         words.append([
             sum(code * base**n for n, code in enumerate(codes[first : first + per_word]))
@@ -766,15 +767,29 @@
     mirrored = level >= depth // 2
     row = jnp.where(mirrored, depth - 1 - level, level)
 
-    def one_word(place, carry):
-        word = 0
-        for at, listing in enumerate(words):
-            for turn, value in enumerate(listing):
-                word = word + jnp.where((row == at) & (place == turn), value, 0)
-
+    depth_bits = (depth - 1).bit_length()
+
+    def chosen_word(turn):
+        level_words = [
+            functools.reduce(
+                lambda found, at: jnp.where(row == at, words[at][n], found),
+                range(1, len(words)), words[0][n],
+            )
+            for n in range(len(words[0]))
+        ]
+        bit = 1
+        while len(level_words) > 1:
+            odd = lax.rem(lax.div(turn, bit), 2) == 1
+            pairs = zip(level_words[::2], level_words[1::2] + level_words[-1:])
+            level_words = [jnp.where(odd, late, soon) for soon, late in pairs]
+            bit *= 2
+        return level_words[0]
+
+    def one_word(turn, carry):
         def one_step(_, rest):
-            code = rest % base
-            kind, at, q = code // (4 * depth), code // 4 % depth, code % 4
+            code = lax.rem(rest, base)
+            kind = lax.div(code, 4 << depth_bits)
+            at, q = lax.rem(lax.div(code, 4), 1 << depth_bits), lax.rem(code, 4)
             at = jnp.where(mirrored, depth - 1 - at, at)
             for first in range(0, len(kinds), 4):
 
@@ -785,9 +800,9 @@
                             functools.partial(actions[kinds[number]], at, q)
                         )
 
-            return rest // base
-
-        lax.fori_loop(0, per_word, one_step, word)
+            return lax.div(rest, base)
+
+        lax.fori_loop(0, per_word, one_step, chosen_word(turn))
         return carry
 
     lax.fori_loop(0, len(words[0]), one_word, 0)

time: 89 us -> 88.7 us (level)
  no operation moved by 1% of the time
where the time goes in v6:
time: 88.7 us; the launch traced here: 88.6 us
  Pallas kernels  86.4 us (97%)
  local copies, waits for them, and re-layouts  1.49 us (2%)
    pallas_call x1, Pallas kernels, dense_plan(): pl.pallas_call(functools.partial(stream_kernel, depth, capacity, experts,...  86.4 us

profile of v6, /device:TPU:0, one launch (start us, length us, event | category | flops | bytes accessed | tf_op | source)
XLA Modules:
  0.0 88.6 jit_solution(15086057491854971653)
XLA Ops:
  0.6 86.4 %shard_map.122 = (bf16[192,1024]{1,0:T(8,128)(2,1)S(1)}, bf16[192,1024]{1,0:T(8,128)(2,1)S(1)}) custom-call(bf16[192,1024]{1,0:T(8,128)(2,1)} %refs_0_.1, f32[1,1024]{1,0:T(1,128)} %bitcast.11, s32[2,192]{1,0:T(2,128)} %bitcast.14, f32[2,192]{1,0:T(2,128)} %bitcast.15, bf16[1024,512]{1,0:T(8,128)(2,1)} %bitcast.8, bf16[1024,512]{1,0:T(8,128)(2,1)} %bitcast.9, ...), custom_call_target="tpu_custom_call" | custom-call | tf_op jit(solution)/shard_map/pallas_call | solution.py:844
  87.1 0.7 copy.15
  87.8 0.7 copy.16
